TPU v7x, 32 devices: a whole 2x2x4 slice. The times are simulated.
32 devices in a mesh: ep: 32 (over z, y, x, core).
Axes of the slice: x: 2, y: 2, z: 4, core: 2. Of those that a mesh axis runs over, the one named last changes fastest.
Arguments:
- tokens: bfloat16 [4096, 2048], P('ep'), may hold values from -6 to 6
- norm_gain: float32 [2048], replicated, may hold values from 0.1 to 1.9
- expert_ids: int32 [4096, 4], P('ep'), may hold values from 0 to 63, as said below
- gate_weights: float32 [4096, 4], P('ep'), may hold values from 0.1 to 0.6
- expert_gate: bfloat16 [64, 2048, 512], P('ep'), may hold values from -0.125 to 0.125
- expert_up: bfloat16 [64, 2048, 512], P('ep'), may hold values from -0.125 to 0.125
- expert_down: bfloat16 [64, 512, 2048], P('ep'), may hold values from -0.25 to 0.25
- shared_gate: bfloat16 [2048, 512], P('ep'), may hold values from -0.125 to 0.125
- shared_up: bfloat16 [2048, 512], P('ep'), may hold values from -0.125 to 0.125
- shared_down: bfloat16 [512, 2048], P(None, 'ep'), may hold values from -0.25 to 0.25
Outputs:
- mixed: bfloat16 [4096, 2048], P('ep')
Inputs may be any that keep to these rules, and one draw needn't show every extreme that they name: `expert_ids`: expert e belongs to device e // 2; each row names 4 experts of 4 different devices; among the rows of one device at most 24 name experts of any one device, hence at most 24 any one expert; in every aligned block of 128 rows exactly 24 rows name one and the same expert.
All inputs are finite; a program needn't handle non-finite values.
Results may differ from a plain program's by a relative error of at most 0.0067.
Values may be sent and summed in bfloat16 or wider, within the bound.
No kernel may reach another device: no remote copies, remote signals or barrier semaphores. Data moves between devices by JAX's collectives and lax.ppermute only.
A program may use at most 128 MiB of HBM per device.

v0:
```python
import jax
import jax.numpy as jnp
from jax import lax
from jax.sharding import PartitionSpec as P

EPS = 1e-06


def normalize(tokens, norm_gain):
    values = tokens.astype(jnp.float32)
    scaled = values * lax.rsqrt(jnp.mean(values * values, axis=-1, keepdims=True) + EPS)
    return (scaled * norm_gain).astype(jnp.bfloat16)


def run_single(w_gate, w_up, w_down, incoming):
    gate_val = jnp.einsum("scd,df->scf", incoming, w_gate, preferred_element_type=jnp.float32)
    up_val = jnp.einsum("scd,df->scf", incoming, w_up, preferred_element_type=jnp.float32)
    hidden = (jax.nn.silu(gate_val) * up_val).astype(jnp.bfloat16)
    return jnp.einsum("scf,fd->scd", hidden, w_down, preferred_element_type=jnp.float32).astype(
        jnp.bfloat16
    )


def run_packed(w_gate, w_up, w_down, incoming):
    rows, which = incoming
    result = jnp.zeros(rows.shape, jnp.bfloat16)
    for local in range(w_gate.shape[0]):
        output = run_single(w_gate[local], w_up[local], w_down[local], rows)
        result = jnp.where((which == local)[:, :, None], output, result)
    return result


def per_device(
    tokens,
    norm_gain,
    expert_ids,
    gate_weights,
    expert_gate,
    expert_up,
    expert_down,
    shared_gate,
    shared_up,
    shared_down,
):
    normed = normalize(tokens, norm_gain)
    count_tok, top = expert_ids.shape
    width = normed.shape[1]
    local_experts = expert_gate.shape[0]
    devices_ep = lax.axis_size("ep")
    mean_rows = count_tok * top // devices_ep
    capacity = mean_rows + mean_rows // 2
    flat_ids = expert_ids.reshape(count_tok * top)
    copies = jnp.repeat(normed, top, axis=0)
    target = flat_ids // local_experts
    one_hot = (target[:, None] == jnp.arange(devices_ep, dtype=jnp.int32)[None, :]).astype(
        jnp.int32
    )
    running = jnp.cumsum(one_hot, axis=0)
    slot_index = jnp.sum(running * one_hot, axis=1) - 1
    position = target * capacity + slot_index
    outgoing = jnp.zeros((devices_ep * capacity, width), jnp.bfloat16).at[position].set(copies)
    labels = (
        jnp.full((devices_ep * capacity,), -1, jnp.int32).at[position].set(flat_ids % local_experts)
    )
    outgoing = outgoing.reshape(devices_ep, capacity, width)
    labels = labels.reshape(devices_ep, capacity)
    results = run_packed(
        expert_gate,
        expert_up,
        expert_down,
        (
            lax.all_to_all(outgoing, "ep", split_axis=0, concat_axis=0, tiled=True),
            lax.all_to_all(labels, "ep", split_axis=0, concat_axis=0, tiled=True),
        ),
    )
    returned = lax.all_to_all(results, "ep", split_axis=0, concat_axis=0, tiled=True)
    returned = returned.reshape(devices_ep * capacity, width)
    picked = returned[position].reshape(count_tok, top, width)
    routed = jnp.sum(picked.astype(jnp.float32) * gate_weights[:, :, None], axis=1)
    gate_val = jnp.dot(
        normed,
        lax.all_gather(shared_gate, "ep", axis=0, tiled=True),
        preferred_element_type=jnp.float32,
    )
    up_val = jnp.dot(
        normed,
        lax.all_gather(shared_up, "ep", axis=0, tiled=True),
        preferred_element_type=jnp.float32,
    )
    shared_hidden = (jax.nn.silu(gate_val) * up_val).astype(jnp.bfloat16)
    shared = jnp.dot(
        shared_hidden,
        lax.all_gather(shared_down, "ep", axis=1, tiled=True),
        preferred_element_type=jnp.float32,
    )
    return (routed + shared).astype(jnp.bfloat16)


def solution(mesh):
    return jax.shard_map(
        per_device,
        mesh=mesh,
        in_specs=(
            P("ep", None),
            P(),
            P("ep", None),
            P("ep", None),
            P("ep", None, None),
            P("ep", None, None),
            P("ep", None, None),
            P("ep", None),
            P("ep", None),
            P(None, "ep"),
        ),
        out_specs=P("ep", None),
        check_vma=False,
    )
```

profile of v0, /device:TPU:0, one launch (start us, length us, event | category | flops | bytes accessed | tf_op | source)
XLA Modules:
  0.0 255.9 jit_solution(11900833095416012076)
XLA Ops:
  6.5 0.8 copy.23
  7.7 1.2 reduce-window.6
  8.9 0.2 slice_reduce_fusion
  9.3 2.4 scatter_custom_fusion
  11.7 0.7 all_to_all.12
  12.4 7.3 %all-to-all-start = ((s32[32,1,24]{2,1,0:T(1,128)}), s32[32,1,24]{2,1,0:T(1,128)S(1)}, u32[]{:S(2)}, u32[]{:S(2)}) async-start(s32[32,1,24]{2,1,0:T(1,128)} %bitcast.3), calls=%async_computation | async-start | bytes 32768 | tf_op jit(solution)/shard_map/all_to_all | solution.py:73
  19.7 1.2 fusion.24
  21.0 1.2 fusion.26
  22.2 0.8 copy-done
  23.0 1.0 broadcast_in_dim.38
  24.1 2.1 reshape.198
  26.1 6.7 %scatter_custom_fusion.1 = bf16[768,2048]{1,0:T(8,128)(2,1)} fusion(s32[512]{0:T(512)S(1)} %bitcast.67, bf16[512,2048]{1,0:T(8,128)(2,1)} %reshape.198, bf16[]{:T(256)} %constant.52.clone.1), kind=kCustom, calls=%fused_computation.27 | custom fusion | bytes 3146240 | tf_op jit(solution)/shard_map/scatter | solution.py:61
  32.8 5.8 %all-to-all-start.1 = ((bf16[32,24,2048]{2,1,0:T(8,128)(2,1)}), bf16[32,24,2048]{2,1,0:T(8,128)(2,1)S(1)}, u32[]{:S(2)}, u32[]{:S(2)}) async-start(bf16[32,24,2048]{2,1,0:T(8,128)(2,1)} %bitcast.5), calls=%async_computation.1 | async-start | bytes 6291456 | tf_op jit(solution)/shard_map/all_to_all | solution.py:72
  38.7 0.7 all-gather.4.cloned.1.call-update
  39.4 0.2 all-gather.8.cloned.1.call-start
  39.6 0.5 all-gather.8.cloned.1.call-update
  40.4 79.4 %all-to-all-done.1 = bf16[32,24,2048]{2,1,0:T(8,128)(2,1)S(1)} async-done(((bf16[32,24,2048]{2,1,0:T(8,128)(2,1)}), bf16[32,24,2048]{2,1,0:T(8,128)(2,1)S(1)}, u32[]{:S(2)}, u32[]{:S(2)}) %all-to-all-start.1) | async-done | bytes 3145760 | tf_op jit(solution)/shard_map/all_to_all | solution.py:72
  119.9 4.7 %fusion.4 = f32[32,24,512]{2,1,0:T(8,128)} fusion(bf16[32,24,2048]{2,1,0:T(8,128)(2,1)S(1)} %all-to-all-done.1, bf16[2,2048,512]{2,1,0:T(8,128)(2,1)} %param.14), kind=kOutput, calls=%fused_computation.12 | convolution fusion | flops 1610612736 | bytes 6815744 | tf_op jit(solution)/shard_map/scd,df->scf/dot_general | solution.py:16
  124.5 7.9 %convolution_convert_fusion = bf16[32,24,2048]{2,1,0:T(8,128)(2,1)} fusion(bf16[2,512,2048]{2,1,0:T(8,128)(2,1)} %param.16, f32[32,24,512]{2,1,0:T(8,128)} %fusion.4, bf16[32,24,2048]{2,1,0:T(8,128)(2,1)S(1)} %all-to-all-done.1, bf16[2,2048,512]{2,1,0:T(8,128)(2,1)} %param.15), kind=kOutput, calls=%fused_computation.4 | convolution fusion | flops 3225157632 | bytes 12058624 | tf_op jit(solution)/shard_map/scf,fd->scd/dot_general | solution.py:19
  132.4 4.6 %fusion.9 = f32[32,24,512]{2,1,0:T(8,128)} fusion(bf16[32,24,2048]{2,1,0:T(8,128)(2,1)S(1)} %all-to-all-done.1, bf16[2,2048,512]{2,1,0:T(8,128)(2,1)} %param.14), kind=kOutput, calls=%fused_computation.17 | convolution fusion | flops 1610612736 | bytes 6815744 | tf_op jit(solution)/shard_map/scd,df->scf/dot_general | solution.py:16
  137.1 8.3 %select_select_fusion = bf16[32,24,2048]{2,1,0:T(8,128)(2,1)} fusion(bf16[32,24,2048]{2,1,0:T(8,128)(2,1)} %convolution_convert_fusion, pred[32,24]{1,0:T(8,128)(4,1)S(1)} %copy.31, pred[32,24]{1,0:T(8,128)(4,1)S(1)} %copy.29, bf16[2,512,2048]{2,1,0:T(8,128)(2,1)} %param.16, f32[32,24,512]{2,1,0:T(8,128)} %fusion.9, ...), kind=kOutput, calls=%fused_computation.6 | convolution fusion | flops 3228303360 | bytes 15205888 | tf_op jit(solution)/shard_map/scf,fd->scd/dot_general | solution.py:19
  145.4 4.1 %all-to-all-start.2 = ((bf16[32,24,2048]{2,1,0:T(8,128)(2,1)}), bf16[32,24,2048]{2,1,0:T(8,128)(2,1)S(1)}, u32[]{:S(2)}, u32[]{:S(2)}) async-start(bf16[32,24,2048]{2,1,0:T(8,128)(2,1)} %select_select_fusion), calls=%async_computation.2 | async-start | bytes 6291456 | tf_op jit(solution)/shard_map/all_to_all | solution.py:76
  149.5 0.3 all-gather.6.cloned.1.call-start
  149.8 0.5 all-gather.6.cloned.1.call-update
  150.2 0.1 copy.32
  150.4 2.2 fusion.49
  152.6 78.1 %all-to-all-done.2 = bf16[32,24,2048]{2,1,0:T(8,128)(2,1)S(1)} async-done(((bf16[32,24,2048]{2,1,0:T(8,128)(2,1)}), bf16[32,24,2048]{2,1,0:T(8,128)(2,1)S(1)}, u32[]{:S(2)}, u32[]{:S(2)}) %all-to-all-start.2) | async-done | bytes 3145760 | tf_op jit(solution)/shard_map/all_to_all | solution.py:76
  230.7 3.3 %gather_fusion = bf16[512,2048]{1,0:T(8,128)(2,1)} fusion(bf16[768,2048]{1,0:T(8,128)(2,1)S(1)} %bitcast.65, s32[1024]{0:T(1024)S(1)} %pad_clamp_fusion), kind=kCustom, calls=%fused_computation | custom fusion | bytes 4196352 | tf_op jit(solution)/shard_map/gather | solution.py:78
  234.0 4.8 %reshape.177 = f32[128,4,2048]{2,1,0:T(4,128)} reshape(bf16[512,2048]{1,0:T(8,128)(2,1)} %gather_fusion) | data formatting | bytes 6291456 | tf_op jit(solution)/shard_map/convert_element_type | solution.py:79
  238.7 5.4 %multiply_reduce_fusion = f32[128,2048]{1,0:T(8,128)S(1)} fusion(f32[128,4,2048]{2,1,0:T(4,128)} %reshape.177, f32[128,4]{1,0:T(8,128)S(1)} %copy.32), kind=kLoop, calls=%fused_computation.3 | loop fusion | flops 1835008 | bytes 5244928 | tf_op jit(solution)/shard_map/reduce_sum | solution.py:79
  244.2 1.0 all-gather.6.cloned.1.call-done
  245.2 4.2 %fusion = bf16[128,2048]{1,0:T(8,128)(2,1)} fusion(f32[128,2048]{1,0:T(8,128)S(1)} %multiply_reduce_fusion, bf16[512,2048]{0,1:T(8,128)(2,1)} %all-gather.8.cloned.1.call-done, bf16[128,2048]{1,0:T(8,128)(2,1)S(1)} %copy-done.1, bf16[2048,512]{1,0:T(8,128)(2,1)} %all-gather.6.cloned.1.call-done, f32[128,512]{1,0:T(8,128)S(1)} %fusion.49), kind=kOutput, calls=%fused_computation.8 | convolution fusion | flops 537788416 | bytes 6553600 | tf_op jit(solution)/shard_map/dot_general | solution.py:91
  (26 shorter events, 0.9 us)
Async XLA Ops:
  12.4 20.4 %all-to-all-start = ((s32[32,1,24]{2,1,0:T(1,128)}), s32[32,1,24]{2,1,0:T(1,128)S(1)}, u32[]{:S(2)}, u32[]{:S(2)}) async-start(s32[32,1,24]{2,1,0:T(1,128)} %bitcast.3), calls=%async_computation | async-start | bytes 32768 | tf_op jit(solution)/shard_map/all_to_all | solution.py:73
  22.2 0.8 copy-start
  32.8 87.0 %all-to-all-start.1 = ((bf16[32,24,2048]{2,1,0:T(8,128)(2,1)}), bf16[32,24,2048]{2,1,0:T(8,128)(2,1)S(1)}, u32[]{:S(2)}, u32[]{:S(2)}) async-start(bf16[32,24,2048]{2,1,0:T(8,128)(2,1)} %bitcast.5), calls=%async_computation.1 | async-start | bytes 6291456 | tf_op jit(solution)/shard_map/all_to_all | solution.py:72
  38.7 111.7 %all-gather.4.cloned.1.call-start = ((), (), s32[]{:S(2)}) async-start(), calls=%async_computation.3 | async-start | bytes 2162688 | tf_op jit(solution)/shard_map/all_gather | solution.py:82
  39.4 204.7 %all-gather.8.cloned.1.call-start = ((), (), s32[]{:S(2)}) async-start(), calls=%async_computation.5 | async-start | bytes 2162688 | tf_op jit(solution)/shard_map/all_gather | solution.py:93
  145.4 4.8 %copy-start.2 = (f32[128,4]{0,1:T(4,128)S(1)}, f32[128,4]{0,1:T(4,128)}, u32[]{:S(2)}) copy-start(f32[128,4]{0,1:T(4,128)} %param.13) | copy-start | bytes 6148
  145.4 85.3 %all-to-all-start.2 = ((bf16[32,24,2048]{2,1,0:T(8,128)(2,1)}), bf16[32,24,2048]{2,1,0:T(8,128)(2,1)S(1)}, u32[]{:S(2)}, u32[]{:S(2)}) async-start(bf16[32,24,2048]{2,1,0:T(8,128)(2,1)} %select_select_fusion), calls=%async_computation.2 | async-start | bytes 6291456 | tf_op jit(solution)/shard_map/all_to_all | solution.py:76
  149.5 95.7 %all-gather.6.cloned.1.call-start = ((), (), s32[]{:S(2)}) async-start(), calls=%async_computation.4 | async-start | bytes 2162688 | tf_op jit(solution)/shard_map/all_gather | solution.py:87
  238.7 6.5 %copy-start.1 = (bf16[128,2048]{1,0:T(8,128)(2,1)S(1)}, bf16[128,2048]{1,0:T(8,128)(2,1)}, u32[]{:S(2)}) copy-start(bf16[128,2048]{1,0:T(8,128)(2,1)} %copy-done) | copy-start | bytes 1572868
Sparse Core Ops, SparseCore 0:
  42.4 67.6 all-gather.3
  112.9 68.7 all-gather.7
  184.5 60.6 all-gather.5
where the time goes:
time: 256 us
  waiting for transfers between devices  160 us (62%)
  matrix products  32 us (12%)
  local copies, waits for them, and re-layouts  23.5 us (9%)
  starting transfers between devices  17.7 us (7%)
  between operations  13.3 us (5%)
  other arithmetic  9.27 us (4%)
    all_to_all x1, waiting for transfers between devices, per_device(): lax.all_to_all(outgoing, 'ep', split_axis=0, concat_axis=0, tiled=True)  79.4 us
    all_to_all x1, waiting for transfers between devices, per_device(): lax.all_to_all(results, 'ep', split_axis=0, concat_axis=0, tiled=True)  78.1 us
    dot_general x2, matrix products, run_single(): jnp.einsum('scf,fd->scd', hidden, w_down, preferred_element_type=jnp.floa...  16.3 us
    dot_general x2, matrix products, run_single(): jnp.einsum('scd,df->scf', incoming, w_gate, preferred_element_type=jnp.fl...  9.29 us
    all_to_all x1, starting transfers between devices, per_device(): lax.all_to_all(labels, 'ep', split_axis=0, concat_axis=0, tiled=True)  7.33 us
    scatter x1, local copies, waits for them, and re-layouts, per_device(): jnp.zeros((devices_ep * capacity, width), jnp.bfloat16).at[position]  6.71 us
    all_to_all x1, starting transfers between devices, per_device(): lax.all_to_all(outgoing, 'ep', split_axis=0, concat_axis=0, tiled=True)  5.83 us
    reduce_sum x1, other arithmetic, per_device(): jnp.sum(picked.astype(jnp.float32) * gate_weights[:, :, None], axis=1)  5.41 us
  transfers between devices with their start and end apart: 6, of which 3 were waited for; matrix products, arithmetic and copies ran while one was open for 21% of the time, Pallas kernels for 0%

commit v1 on v0

v1 whole, which is shorter than its diff:
```python
import functools

import jax
import jax.numpy as jnp
from jax import lax
from jax.experimental import pallas as pl
from jax.experimental.pallas import tpu as pltpu
from jax.sharding import PartitionSpec as P


EPS = 1e-06
LANES = 128
F32 = jnp.float32
BF16 = jnp.bfloat16


VMEM = pl.BlockSpec(memory_space=pltpu.VMEM)
SMEM = pl.BlockSpec(memory_space=pltpu.SMEM)


def routes(place_ref, ids_ref, weights_ref, local_experts, slots, cap):
    top, count = ids_ref.shape
    rows = slots * cap
    ids = ids_ref[...]
    weights = weights_ref[...]
    target = ids // local_experts
    local = (ids % local_experts).astype(F32)
    device = place_ref[0] + (
        lax.broadcasted_iota(jnp.int32, (slots, count), 0) ^ place_ref[1]
    )
    zero = jnp.zeros((slots, count), F32)
    member, weight, label = zero, zero, zero
    for k in range(top):
        hit = target[k : k + 1, :] == device
        member = jnp.where(hit, 1.0, member)
        weight = jnp.where(hit, weights[k : k + 1, :], weight)
        label = jnp.where(hit, local[k : k + 1, :], label)
    square = lambda dim: lax.broadcasted_iota(jnp.int32, (count, count), dim)
    before = (square(0) < square(1)).astype(BF16)
    rank = jnp.dot(member.astype(BF16), before, preferred_element_type=F32)
    rank = jnp.where(member > 0.0, rank, -1.0)
    row = lax.broadcasted_iota(jnp.int32, (rows, slots), 0)
    expand = (row // cap == lax.broadcasted_iota(jnp.int32, (rows, slots), 1)).astype(BF16)
    spread = lambda array: jnp.dot(expand, array.astype(BF16), preferred_element_type=F32)
    want = (lax.broadcasted_iota(jnp.int32, (rows, count), 0) % cap).astype(F32)
    pick = (spread(rank) == want).astype(F32)
    labels = jnp.sum(pick * spread(label), axis=1, keepdims=True)
    labels = jnp.broadcast_to(labels, (rows, LANES)).astype(BF16)
    high = weight.astype(BF16).astype(F32)
    mix = jnp.concatenate([(pick * spread(high)).T, (pick * spread(weight - high)).T], axis=0)
    return pick.astype(BF16), labels, mix.astype(BF16)


def norm_kernel(tokens_ref, gain_ref, out_ref):
    values = tokens_ref[...].astype(F32)
    scale = lax.rsqrt(jnp.mean(values * values, axis=-1, keepdims=True) + EPS)
    out_ref[...] = (values * scale * gain_ref[...]).astype(BF16)


def front_kernel(place_ref, ids_ref, weights_ref, x_ref, mix_ref, *out_refs, **sizes):
    pick, labels, mix = routes(place_ref, ids_ref, weights_ref, **sizes)
    mix_ref[...] = mix
    width = x_ref.shape[1]
    cap = sizes["cap"]
    sent = jnp.dot(pick, x_ref[...], preferred_element_type=F32).astype(BF16)
    for slot, out_ref in enumerate(out_refs):
        out_ref[:, :width] = sent[slot * cap : (slot + 1) * cap]
        out_ref[:, width:] = labels[slot * cap : (slot + 1) * cap]


def route_kernel(place_ref, ids_ref, weights_ref, pick_ref, label_ref, mix_ref, **sizes):
    pick_ref[...], label_ref[...], mix_ref[...] = routes(
        place_ref, ids_ref, weights_ref, **sizes
    )


def gather_kernel(pick_ref, label_ref, x_ref, out_ref):
    width = x_ref.shape[1]
    out_ref[:, :width] = jnp.dot(pick_ref[...], x_ref[...], preferred_element_type=F32).astype(
        BF16
    )
    out_ref[:, width:] = label_ref[...]


def join(refs, rows_ref):
    start = 0
    for ref in refs:
        rows_ref[start : start + ref.shape[0], :] = ref[...]
        start += ref.shape[0]


def combined(mix_ref, back_ref):
    both = jnp.dot(mix_ref[...], back_ref[...], preferred_element_type=F32)
    count = both.shape[0] // 2
    return both[:count] + both[count:]


def combine_kernel(mix_ref, back_ref, shared_ref, out_ref):
    out_ref[...] = (combined(mix_ref, back_ref) + shared_ref[...]).astype(BF16)


def own_kernel(mix_ref, shared_ref, *refs):
    *back_refs, out_ref, rows_ref = refs
    join(back_refs, rows_ref)
    out_ref[...] = combined(mix_ref, rows_ref) + shared_ref[...]


def add_kernel(own_ref, other_ref, out_ref):
    out_ref[...] = (own_ref[...] + other_ref[...].astype(F32)).astype(BF16)


def expert_kernel(gate_ref, up_ref, down_ref, *refs, pieces, cuts, outs):
    in_refs, out_refs = refs[:pieces], refs[pieces : 2 * pieces]
    gate_buf, up_buf, down_buf, hidden_ref, sems, *rest = refs[2 * pieces :]
    rows_ref = rest[0] if rest else in_refs[0]
    experts, width, hidden = gate_ref.shape
    block = hidden // cuts
    parts = [(e, pl.ds(j * block, block)) for e in range(experts) for j in range(cuts)]
    firsts = []
    for i, (e, cols) in enumerate(parts):
        pair = [
            pltpu.make_async_copy(src.at[e, :, cols], dst.at[i], sems.at[k, i])
            for k, (src, dst) in enumerate(((gate_ref, gate_buf), (up_ref, up_buf)))
        ]
        for copy in pair:
            copy.start()
        firsts.append(pair)
    piece = width // outs
    seconds = []
    for i in range(outs):
        cols = pl.ds(i * piece, piece)
        copy = pltpu.make_async_copy(down_ref.at[:, cols], down_buf.at[i], sems.at[2, i])
        copy.start()
        seconds.append(copy)
    if rest:
        join(in_refs, rows_ref)
    for i, (e, _) in enumerate(parts):
        for copy in firsts[i]:
            copy.wait()
        rows = rows_ref[:, :width]
        mine = rows_ref[:, width:][:, :1].astype(F32) == float(e)
        gate_val = jnp.dot(rows, gate_buf[i], preferred_element_type=F32)
        up_val = jnp.dot(rows, up_buf[i], preferred_element_type=F32)
        value = jnp.where(mine, gate_val / (1.0 + jnp.exp(-gate_val)) * up_val, 0.0)
        hidden_ref[:, i * block : (i + 1) * block] = value.astype(BF16)
    for i, copy in enumerate(seconds):
        copy.wait()
        result = jnp.dot(
            hidden_ref[...], down_buf[i], preferred_element_type=F32
        ).astype(BF16)
        start = 0
        for out_ref in out_refs:
            stop = start + out_ref.shape[0]
            out_ref[:, i * piece : (i + 1) * piece] = result[start:stop]
            start = stop


def run_experts(rows, w_gate, w_up, w_down):
    experts, width, hidden = w_gate.shape
    cuts, outs = 2, 2
    steps = experts * cuts
    block, piece = hidden // cuts, width // outs
    count = sum(part.shape[0] for part in rows)
    scratch = [
        pltpu.VMEM((steps, width, block), BF16),
        pltpu.VMEM((steps, width, block), BF16),
        pltpu.VMEM((outs, experts * hidden, piece), BF16),
        pltpu.VMEM((count, experts * hidden), BF16),
        pltpu.SemaphoreType.DMA((3, max(steps, outs))),
    ]
    if len(rows) > 1:
        scratch.append(pltpu.VMEM((count, rows[0].shape[1]), BF16))
    return pl.pallas_call(
        functools.partial(expert_kernel, pieces=len(rows), cuts=cuts, outs=outs),
        in_specs=[pl.BlockSpec(memory_space=pltpu.HBM)] * 3 + [VMEM] * len(rows),
        out_specs=[VMEM] * len(rows),
        out_shape=[jax.ShapeDtypeStruct((part.shape[0], width), BF16) for part in rows],
        scratch_shapes=scratch,
        cost_estimate=pl.CostEstimate(
            flops=6 * count * experts * width * hidden,
            bytes_accessed=6 * experts * width * hidden + 4 * count * width,
            transcendentals=count * experts * hidden,
        ),
        compiler_params=pltpu.CompilerParams(vmem_limit_bytes=60 << 20),
    )(w_gate, w_up, w_down.reshape(experts * hidden, width), *rows)


def shared_kernel(me_ref, parts_ref, own_ref, other_ref, out_own_ref, out_other_ref,
                  gate_ref, up_ref, down_ref, *, offsets):
    me = me_ref[0]
    block = parts_ref.shape[2]
    for place, offset in enumerate(offsets):
        start = pl.multiple_of((me ^ offset) * block, block)
        gate_ref[pl.ds(start, block), :] = parts_ref[place, 0]
        up_ref[pl.ds(start, block), :] = parts_ref[place, 1]
        down_ref[pl.ds(start, block), :] = parts_ref[place, 2]
    for x_ref, out_ref in ((own_ref, out_own_ref), (other_ref, out_other_ref)):
        x = x_ref[...]
        gate_val = jnp.dot(x, gate_ref[...], preferred_element_type=F32)
        up_val = jnp.dot(x, up_ref[...], preferred_element_type=F32)
        hidden = (gate_val / (1.0 + jnp.exp(-gate_val)) * up_val).astype(BF16)
        out_ref[...] = lax.dot_general(
            hidden, down_ref[...], (((1,), (1,)), ((), ())), preferred_element_type=F32
        )


def call(kernel, out, args, scalars=1, flops=0, vmem=24, **options):
    shapes = jax.tree.leaves(out)
    specs = jax.tree.map(lambda _: VMEM, out)
    return pl.pallas_call(
        kernel,
        in_specs=[SMEM] * scalars + [VMEM] * (len(args) - scalars),
        out_specs=specs,
        out_shape=out,
        cost_estimate=pl.CostEstimate(
            flops=flops,
            bytes_accessed=sum(a.size * a.dtype.itemsize for a in list(args) + shapes),
            transcendentals=0,
        ),
        compiler_params=pltpu.CompilerParams(vmem_limit_bytes=vmem << 20),
        **options,
    )(*args)


def per_device(
    tokens,
    norm_gain,
    expert_ids,
    gate_weights,
    expert_gate,
    expert_up,
    expert_down,
    shared_gate,
    shared_up,
    shared_down,
):
    devices = lax.axis_size("ep")
    me = lax.axis_index("ep").astype(jnp.int32)
    half = devices // 2
    side = me // half
    count, top = expert_ids.shape
    width = tokens.shape[1]
    mean_rows = count * top // devices
    cap = -(-(mean_rows + mean_rows // 2) // 8) * 8
    rows = half * cap
    sizes = dict(local_experts=expert_gate.shape[0], slots=half, cap=cap)
    groups = [list(range(half)), list(range(half, devices))]

    def exchange(array, bit):
        return lax.ppermute(array, "ep", [(i, i ^ bit) for i in range(devices)])

    def within(array):
        return lax.all_to_all(array, "ep", 0, 0, axis_index_groups=groups, tiled=True)

    base = side * half
    place = jnp.stack([base, me % half])
    place_other = jnp.stack([base, jnp.zeros_like(me)])
    dense = jax.ShapeDtypeStruct((count, width), BF16)
    plan = (
        jax.ShapeDtypeStruct((rows, count), BF16),
        jax.ShapeDtypeStruct((rows, LANES), BF16),
        jax.ShapeDtypeStruct((2 * count, rows), BF16),
    )
    sent = jax.ShapeDtypeStruct((rows, width + LANES), BF16)
    work = 2 * rows * count * width
    few = 8 * rows * count * half

    parts = jnp.stack([shared_gate, shared_up, shared_down.T])[None]
    cut = parts.shape[3] // 2
    offsets = [0]
    for bit in shared_steps(devices):
        if bit == half:
            low, high = parts[..., :cut], parts[..., cut:]
            mine = jnp.where(side == 0, low, high)
            theirs = jnp.where(side == 0, high, low)
        else:
            mine = theirs = parts
        parts = jnp.concatenate([mine, exchange(theirs, bit)], axis=0)
        offsets += [offset ^ bit for offset in offsets]

    ids, weights = expert_ids.T, gate_weights.T
    ids_other = exchange(ids, half)
    weights_other = exchange(weights, half)
    piece = jax.ShapeDtypeStruct((cap, width + LANES), BF16)
    normed = call(
        norm_kernel, dense, (tokens, norm_gain.reshape(1, width)),
        scalars=0, flops=8 * count * width,
    )
    normed_other = exchange(normed, half)
    mix, *outgoing = call(
        functools.partial(front_kernel, **sizes), [plan[2]] + [piece] * half,
        (place, ids, weights, normed), flops=work + few,
    )
    incoming = [outgoing[0]] + [exchange(outgoing[r], r) for r in range(1, half)]
    pick, label, mix_other = call(
        functools.partial(route_kernel, **sizes), plan,
        (place_other, ids_other, weights_other), flops=few,
    )
    outgoing_other = call(gather_kernel, sent, (pick, label, normed_other), scalars=0, flops=work)
    incoming_other = within(outgoing_other)
    results = run_experts(incoming, expert_gate, expert_up, expert_down)
    (results_other,) = run_experts([incoming_other], expert_gate, expert_up, expert_down)
    back_other = within(results_other)
    back = [results[0]] + [exchange(results[r], r) for r in range(1, half)]

    block = shared_gate.shape[0]
    full = pltpu.VMEM((devices * block, cut), BF16)
    shape = jax.ShapeDtypeStruct((count, width), F32)
    shared_own, shared_other = call(
        functools.partial(shared_kernel, offsets=tuple(offsets)),
        (shape, shape),
        (me.reshape(1), parts, normed, normed_other),
        flops=12 * count * width * cut,
        scratch_shapes=[full, full, full],
    )
    partial = call(
        combine_kernel, dense, (mix_other, back_other, shared_other),
        scalars=0, flops=2 * work,
    )
    from_other = exchange(partial, half)
    total = call(
        own_kernel, shape, (mix, shared_own, *back),
        scalars=0, flops=2 * work, scratch_shapes=[pltpu.VMEM((rows, width), BF16)],
    )
    return call(add_kernel, dense, (total, from_other), scalars=0, flops=count * width)


def shared_steps(devices):
    half = devices // 2
    bits = [1 << b for b in range(devices.bit_length() - 3, -1, -1)]
    early = [bit for bit in bits if 2 <= bit <= 4]
    late = [bit for bit in bits if 4 < bit]
    return early + [half] + late + [1]


def solution(mesh):
    return jax.shard_map(
        per_device,
        mesh=mesh,
        in_specs=(
            P("ep", None),
            P(),
            P("ep", None),
            P("ep", None),
            P("ep", None, None),
            P("ep", None, None),
            P("ep", None, None),
            P("ep", None),
            P("ep", None),
            P(None, "ep"),
        ),
        out_specs=P("ep", None),
        check_vma=False,
    )
```

time: 256 us -> 214 us (0.84)
  waiting for transfers between devices: 160 us -> 106 us
  starting transfers between devices: 17.7 us -> 64.1 us
  matrix products: 32 us -> 0 us
  Pallas kernels: 0 us -> 28.8 us
  local copies, waits for them, and re-layouts: 23.5 us -> 6.83 us
  between operations: 13.3 us -> 0.33 us
    all_to_all x3 -> x2, waiting for transfers between devices: 157 us -> 0.01 us  [within(): lax.all_to_all(array, 'ep', 0, 0, axis_index_groups=groups, tiled=True)]
    ppermute x0 -> x39, waiting for transfers between devices: none -> 106 us  [exchange(): return lax.ppermute(array, 'ep', [(i, i ^ bit) for i in range(devices)])]
    ppermute x0 -> x39, starting transfers between devices: none -> 55.5 us  [exchange(): return lax.ppermute(array, 'ep', [(i, i ^ bit) for i in range(devices)])]
    dot_general x6 -> x0, matrix products: 32 us -> none  [the longest x2 16.3 us: run_single(): jnp.einsum('scf,fd->scd', hidden, w_down, preferred_element_type=jnp.floa...]
    pallas_call x0 -> x10, Pallas kernels: none -> 28.8 us  [the longest x2 20.5 us: run_experts(): pl.pallas_call(functools.partial(expert_kernel, pieces=len(rows), cuts=cu...]
    scatter x2 -> x0, local copies, waits for them, and re-layouts: 9.16 us -> none  [the longest x1 6.71 us: per_device(): jnp.zeros((devices_ep * capacity, width), jnp.bfloat16).at[position]]
    all_to_all x3 -> x2, starting transfers between devices: 17.2 us -> 8.58 us  [within(): lax.all_to_all(array, 'ep', 0, 0, axis_index_groups=groups, tiled=True)]
    reduce_sum x3 -> x0, other arithmetic: 6.75 us -> none  [the longest x1 5.41 us: per_device(): jnp.sum(picked.astype(jnp.float32) * gate_weights[:, :, None], axis=1)]
  transfers between devices with their start and end apart: 6 -> 41, of which waited for: 3 -> 17; matrix products, arithmetic and copies ran while one was open for 21% -> 3% of each run, Pallas kernels for 0% -> 12%
where the time goes in v1:
time: 214 us; the launch traced here: 213 us
  waiting for transfers between devices  106 us (50%)
  starting transfers between devices  64.1 us (30%)
  Pallas kernels  28.8 us (13%)
  local copies, waits for them, and re-layouts  6.83 us (3%)
  other arithmetic  6.76 us (3%)
    ppermute x39, waiting for transfers between devices, exchange(): return lax.ppermute(array, 'ep', [(i, i ^ bit) for i in range(devices)])  106 us
    ppermute x39, starting transfers between devices, exchange(): return lax.ppermute(array, 'ep', [(i, i ^ bit) for i in range(devices)])  55.5 us
    pallas_call x2, Pallas kernels, run_experts(): pl.pallas_call(functools.partial(expert_kernel, pieces=len(rows), cuts=cu...  20.5 us
    all_to_all x2, starting transfers between devices, within(): lax.all_to_all(array, 'ep', 0, 0, axis_index_groups=groups, tiled=True)  8.58 us
    pallas_call x8, Pallas kernels, call(): pl.pallas_call(kernel, in_specs=[SMEM] * scalars + [VMEM] * (len(args) -...  8.29 us
    unnamed x50, local copies, waits for them, and re-layouts  6.83 us
    concatenate x5, other arithmetic, per_device(): parts = jnp.concatenate([mine, exchange(theirs, bit)], axis=0)  5.79 us
  transfers between devices with their start and end apart: 41, of which 17 were waited for; matrix products, arithmetic and copies ran while one was open for 3% of the time, Pallas kernels for 12%

profile of v1, /device:TPU:0, one launch (start us, length us, event | category | flops | bytes accessed | tf_op | source)
XLA Modules:
  0.0 213.2 jit_solution(13611516686296229777)
XLA Ops:
  2.0 4.1 %collective-permute-start.5 = (bf16[128,2048]{1,0:T(8,128)(2,1)S(1)}, bf16[128,2048]{1,0:T(8,128)(2,1)S(1)}, u32[]{:S(2)}, u32[]{:S(2)}) collective-permute-start(bf16[128,2048]{1,0:T(8,128)(2,1)S(1)} %shard_map.100.x_ref.own_ref), channel_id=1, source_target_pairs={{0,16},{1,17},{2,18},{3,19},{4,20},{5,21},{6,22},{7,23},{8,24},{9,... | collective-permute-start | bytes 1572872 | tf_op jit(solution)/shard_map/ppermute | solution.py:250
  6.2 2.8 %collective-permute-start.37 = (f32[4,128]{1,0:T(4,128)}, f32[4,128]{1,0:T(4,128)S(1)}, u32[]{:S(2)}, u32[]{:S(2)}) collective-permute-start(f32[4,128]{1,0:T(4,128)} %bitcast.22), channel_id=1, source_target_pairs={{0,16},{1,17},{2,18},{3,19},{4,20},{5,21},{6,22},{7,23},{8,24},{9,... | collective-permute-start | bytes 6152 | tf_op jit(solution)/shard_map/ppermute | solution.py:250
  9.1 20.3 %collective-permute-done.36.ids_ref = s32[4,128]{1,0:T(4,128)S(1)} collective-permute-done((s32[4,128]{1,0:T(4,128)}, s32[4,128]{1,0:T(4,128)S(1)}, u32[]{:S(2)}, u32[]{:S(2)}) %collective-permute-start.36) | collective-permute-done | bytes 2080 | tf_op jit(solution)/shard_map/ppermute | solution.py:250
  30.5 1.7 shard_map.106
  32.2 4.5 %all-to-all-start = ((bf16[16,24,2176]{2,1,0:T(8,128)(2,1)}), bf16[16,24,2176]{2,1,0:T(8,128)(2,1)}, u32[]{:S(2)}, u32[]{:S(2)}) async-start(bf16[16,24,2176]{2,1,0:T(8,128)(2,1)} %bitcast.12), calls=%async_computation | async-start | bytes 3342336 | tf_op jit(solution)/shard_map/all_to_all | solution.py:253
  36.8 1.8 collective-permute-start
  38.7 23.2 %collective-permute-done = bf16[1,3,64,512]{3,2,1,0:T(8,128)(2,1)S(1)} collective-permute-done((bf16[1,3,64,512]{3,2,1,0:T(8,128)(2,1)S(1)}, bf16[1,3,64,512]{3,2,1,0:T(8,128)(2,1)S(1)}, u32[]{:S(2)}, u32[]{:S(2)}) %collective-permute-start) | collective-permute-done | bytes 196640 | tf_op jit(solution)/shard_map/ppermute | solution.py:250
  61.9 1.5 collective-permute-start.1
  63.4 9.3 %collective-permute-done.1 = bf16[2,3,64,512]{3,2,1,0:T(8,128)(2,1)S(1)} collective-permute-done((bf16[2,3,64,512]{3,2,1,0:T(8,128)(2,1)S(1)}, bf16[2,3,64,512]{3,2,1,0:T(8,128)(2,1)S(1)}, u32[]{:S(2)}, u32[]{:S(2)}) %collective-permute-start.1) | collective-permute-done | bytes 393248 | tf_op jit(solution)/shard_map/ppermute | solution.py:250
  73.6 3.1 %collective-permute-start.2 = (bf16[4,3,64,256]{3,2,1,0:T(8,128)(2,1)}, bf16[4,3,64,256]{3,2,1,0:T(8,128)(2,1)}, u32[]{:S(2)}, u32[]{:S(2)}) collective-permute-start(bf16[4,3,64,256]{3,2,1,0:T(8,128)(2,1)} %get-tuple-element.82), channel_id=1, source_target_pairs={{0,16},{1,17},{2,18},{3,19},{4,20},{5,21},{6,22},{7,23},{8,24},{9,... | collective-permute-start | bytes 1179656 | tf_op jit(solution)/shard_map/ppermute | solution.py:250
  76.7 10.2 %shard_map.107 = bf16[384,2048]{1,0:T(8,128)(2,1)} custom-call(bf16[2,2048,512]{2,1,0:T(8,128)(2,1)} %gate_ref.3, bf16[2,2048,512]{2,1,0:T(8,128)(2,1)} %up_ref.3, bf16[1024,2048]{1,0:T(8,128)(2,1)} %bitcast.28, bf16[384,2176]{1,0:T(8,128)(2,1)} %bitcast.13.refs_0_), custom_call_target="tpu_custom_call" | custom-call | flops 4831838208 | bytes 15728640 | tf_op jit(solution)/shard_map/pallas_call | solution.py:173
  87.0 4.0 %all-to-all-start.1 = ((bf16[16,24,2048]{2,1,0:T(8,128)(2,1)}), bf16[16,24,2048]{2,1,0:T(8,128)(2,1)S(1)}, u32[]{:S(2)}, u32[]{:S(2)}) async-start(bf16[16,24,2048]{2,1,0:T(8,128)(2,1)} %bitcast.24), calls=%async_computation.1 | async-start | bytes 3145728 | tf_op jit(solution)/shard_map/all_to_all | solution.py:253
  91.0 2.7 %collective-permute-done.2 = bf16[4,3,64,256]{3,2,1,0:T(8,128)(2,1)} collective-permute-done((bf16[4,3,64,256]{3,2,1,0:T(8,128)(2,1)}, bf16[4,3,64,256]{3,2,1,0:T(8,128)(2,1)}, u32[]{:S(2)}, u32[]{:S(2)}) %collective-permute-start.2) | collective-permute-done | bytes 393248 | tf_op jit(solution)/shard_map/ppermute | solution.py:250
  95.6 32.3 %collective-permute-done.3 = bf16[8,3,64,256]{3,2,1,0:T(8,128)(2,1)S(1)} collective-permute-done((bf16[8,3,64,256]{3,2,1,0:T(8,128)(2,1)S(1)}, bf16[8,3,64,256]{3,2,1,0:T(8,128)(2,1)S(1)}, u32[]{:S(2)}, u32[]{:S(2)}) %collective-permute-start.3) | collective-permute-done | bytes 786464 | tf_op jit(solution)/shard_map/ppermute | solution.py:250
  127.9 2.6 %pad_maximum_fusion.1 = bf16[16,3,64,256]{3,2,1,0:T(8,128)(2,1)} fusion(bf16[8,3,64,256]{3,2,1,0:T(8,128)(2,1)S(1)} %collective-permute-done.3, bf16[4,3,64,256]{3,2,1,0:T(8,128)(2,1)} %collective-permute-done.2, bf16[4,3,64,256]{3,2,1,0:T(8,128)(2,1)S(1)} %get-tuple-element.81), kind=kLoop, calls=%fused_computation.1 | loop fusion | flops 1572864 | bytes 3145728 | tf_op jit(solution)/shard_map/concatenate | solution.py:278
  132.6 2.7 %collective-permute-start.10 = (bf16[24,2176]{1,0:T(8,128)(2,1)S(1)}, bf16[24,2176]{1,0:T(8,128)(2,1)S(1)}, u32[]{:S(2)}, u32[]{:S(2)}) collective-permute-start(bf16[24,2176]{1,0:T(8,128)(2,1)S(1)} %get-tuple-element.50), channel_id=1, source_target_pairs={{0,5},{1,4},{2,7},{3,6},{4,1},{5,0},{6,3},{7,2},{8,13},{9,12},{10,... | collective-permute-start | bytes 313352 | tf_op jit(solution)/shard_map/ppermute | solution.py:250
  137.6 4.9 %collective-permute-done.10.refs_5_ = bf16[24,2176]{1,0:T(8,128)(2,1)S(1)} collective-permute-done((bf16[24,2176]{1,0:T(8,128)(2,1)S(1)}, bf16[24,2176]{1,0:T(8,128)(2,1)S(1)}, u32[]{:S(2)}, u32[]{:S(2)}) %collective-permute-start.10) | collective-permute-done | bytes 104480 | tf_op jit(solution)/shard_map/ppermute | solution.py:250
  142.4 3.3 %collective-permute-start.15 = (bf16[24,2176]{1,0:T(8,128)(2,1)S(1)}, bf16[24,2176]{1,0:T(8,128)(2,1)S(1)}, u32[]{:S(2)}, u32[]{:S(2)}) collective-permute-start(bf16[24,2176]{1,0:T(8,128)(2,1)S(1)} %get-tuple-element.55), channel_id=1, source_target_pairs={{0,10},{1,11},{2,8},{3,9},{4,14},{5,15},{6,12},{7,13},{8,2},{9,3},... | collective-permute-start | bytes 313352 | tf_op jit(solution)/shard_map/ppermute | solution.py:250
  145.8 2.2 %collective-permute-start.17 = (bf16[24,2176]{1,0:T(8,128)(2,1)S(1)}, bf16[24,2176]{1,0:T(8,128)(2,1)S(1)}, u32[]{:S(2)}, u32[]{:S(2)}) collective-permute-start(bf16[24,2176]{1,0:T(8,128)(2,1)S(1)} %get-tuple-element.57), channel_id=1, source_target_pairs={{0,12},{1,13},{2,14},{3,15},{4,8},{5,9},{6,10},{7,11},{8,4},{9,5},... | collective-permute-start | bytes 313352 | tf_op jit(solution)/shard_map/ppermute | solution.py:250
  149.0 2.9 %collective-permute-start.19 = (bf16[24,2176]{1,0:T(8,128)(2,1)S(1)}, bf16[24,2176]{1,0:T(8,128)(2,1)S(1)}, u32[]{:S(2)}, u32[]{:S(2)}) collective-permute-start(bf16[24,2176]{1,0:T(8,128)(2,1)S(1)} %get-tuple-element.59), channel_id=1, source_target_pairs={{0,14},{1,15},{2,12},{3,13},{4,10},{5,11},{6,8},{7,9},{8,6},{9,7},... | collective-permute-start | bytes 313352 | tf_op jit(solution)/shard_map/ppermute | solution.py:250
  151.9 2.0 pad_maximum_fusion.parts_ref
  158.8 2.3 %collective-permute-done.19.refs_14_ = bf16[24,2176]{1,0:T(8,128)(2,1)S(1)} collective-permute-done((bf16[24,2176]{1,0:T(8,128)(2,1)S(1)}, bf16[24,2176]{1,0:T(8,128)(2,1)S(1)}, u32[]{:S(2)}, u32[]{:S(2)}) %collective-permute-start.19) | collective-permute-done | bytes 104480 | tf_op jit(solution)/shard_map/ppermute | solution.py:250
  161.8 1.7 shard_map.102
  167.4 3.3 %collective-permute-start.38 = (bf16[128,2048]{1,0:T(8,128)(2,1)S(1)}, bf16[128,2048]{1,0:T(8,128)(2,1)S(1)}, u32[]{:S(2)}, u32[]{:S(2)}) collective-permute-start(bf16[128,2048]{1,0:T(8,128)(2,1)S(1)} %shard_map.108), channel_id=1, source_target_pairs={{0,16},{1,17},{2,18},{3,19},{4,20},{5,21},{6,22},{7,23},{8,24},{9,... | collective-permute-start | bytes 1572872 | tf_op jit(solution)/shard_map/ppermute | solution.py:250
  170.8 10.3 %shard_map.103 = (bf16[24,2048]{1,0:T(8,128)(2,1)}, bf16[24,2048]{1,0:T(8,128)(2,1)}, bf16[24,2048]{1,0:T(8,128)(2,1)}, bf16[24,2048]{1,0:T(8,128)(2,1)}, bf16[2...) custom-call(bf16[2,2048,512]{2,1,0:T(8,128)(2,1)} %gate_ref.3, ...), custom_call_target="tpu_custom_call" | custom-call | flops 4831838208 | bytes 15728640 | tf_op jit(solution)/shard_map/pallas_call | solution.py:173
  184.8 2.4 %collective-permute-done.22.refs_2_ = bf16[24,2048]{1,0:T(8,128)(2,1)S(1)} collective-permute-done((bf16[24,2048]{1,0:T(8,128)(2,1)}, bf16[24,2048]{1,0:T(8,128)(2,1)S(1)}, u32[]{:S(2)}, u32[]{:S(2)}) %collective-permute-start.22) | collective-permute-done | bytes 98336 | tf_op jit(solution)/shard_map/ppermute | solution.py:250
  191.0 2.0 collective-permute-start.29
  194.7 1.8 collective-permute-start.31
  197.6 1.6 collective-permute-start.33
  200.1 2.6 %collective-permute-start.34 = (bf16[24,2048]{1,0:T(8,128)(2,1)}, bf16[24,2048]{1,0:T(8,128)(2,1)S(1)}, u32[]{:S(2)}, u32[]{:S(2)}) collective-permute-start(bf16[24,2048]{1,0:T(8,128)(2,1)} %get-tuple-element.75), channel_id=1, source_target_pairs={{0,14},{1,15},{2,12},{3,13},{4,10},{5,11},{6,8},{7,9},{8,6},{9,7},... | collective-permute-start | bytes 294920 | tf_op jit(solution)/shard_map/ppermute | solution.py:250
  205.9 2.5 %collective-permute-done.34.refs_14_ = bf16[24,2048]{1,0:T(8,128)(2,1)S(1)} collective-permute-done((bf16[24,2048]{1,0:T(8,128)(2,1)}, bf16[24,2048]{1,0:T(8,128)(2,1)S(1)}, u32[]{:S(2)}, u32[]{:S(2)}) %collective-permute-start.34) | collective-permute-done | bytes 98336 | tf_op jit(solution)/shard_map/ppermute | solution.py:250
  208.4 2.3 %collective-permute-done.35.refs_15_ = bf16[24,2048]{1,0:T(8,128)(2,1)S(1)} collective-permute-done((bf16[24,2048]{1,0:T(8,128)(2,1)}, bf16[24,2048]{1,0:T(8,128)(2,1)S(1)}, u32[]{:S(2)}, u32[]{:S(2)}) %collective-permute-start.35) | collective-permute-done | bytes 98336 | tf_op jit(solution)/shard_map/ppermute | solution.py:250
  (119 shorter events, 37.6 us)
Async XLA Ops:
  2.0 28.5 %collective-permute-start.5 = (bf16[128,2048]{1,0:T(8,128)(2,1)S(1)}, bf16[128,2048]{1,0:T(8,128)(2,1)S(1)}, u32[]{:S(2)}, u32[]{:S(2)}) collective-permute-start(bf16[128,2048]{1,0:T(8,128)(2,1)S(1)} %shard_map.100.x_ref.own_ref), channel_id=1, source_target_pairs={{0,16},{1,17},{2,18},{3,19},{4,20},{5,21},{6,22},{7,23},{8,24},{9,... | collective-permute-start | bytes 1572872 | tf_op jit(solution)/shard_map/ppermute | solution.py:250
  6.1 23.3 %collective-permute-start.36 = (s32[4,128]{1,0:T(4,128)}, s32[4,128]{1,0:T(4,128)S(1)}, u32[]{:S(2)}, u32[]{:S(2)}) collective-permute-start(s32[4,128]{1,0:T(4,128)} %bitcast.20), channel_id=1, source_target_pairs={{0,16},{1,17},{2,18},{3,19},{4,20},{5,21},{6,22},{7,23},{8,24},{9,... | collective-permute-start | bytes 6152 | tf_op jit(solution)/shard_map/ppermute | solution.py:250
  6.2 23.3 %collective-permute-start.37 = (f32[4,128]{1,0:T(4,128)}, f32[4,128]{1,0:T(4,128)S(1)}, u32[]{:S(2)}, u32[]{:S(2)}) collective-permute-start(f32[4,128]{1,0:T(4,128)} %bitcast.22), channel_id=1, source_target_pairs={{0,16},{1,17},{2,18},{3,19},{4,20},{5,21},{6,22},{7,23},{8,24},{9,... | collective-permute-start | bytes 6152 | tf_op jit(solution)/shard_map/ppermute | solution.py:250
  32.2 44.5 %all-to-all-start = ((bf16[16,24,2176]{2,1,0:T(8,128)(2,1)}), bf16[16,24,2176]{2,1,0:T(8,128)(2,1)}, u32[]{:S(2)}, u32[]{:S(2)}) async-start(bf16[16,24,2176]{2,1,0:T(8,128)(2,1)} %bitcast.12), calls=%async_computation | async-start | bytes 3342336 | tf_op jit(solution)/shard_map/all_to_all | solution.py:253
  36.8 25.0 %collective-permute-start = (bf16[1,3,64,512]{3,2,1,0:T(8,128)(2,1)S(1)}, bf16[1,3,64,512]{3,2,1,0:T(8,128)(2,1)S(1)}, u32[]{:S(2)}, u32[]{:S(2)}) collective-permute-start(bf16[1,3,64,512]{3,2,1,0:T(8,128)(2,1)S(1)} %maximum_bitcast_fusion), channel_id=1, source_target_pairs={{0,4},{1,5},{2,6},{3,7},{4,0},{5,1},{6,2},{7,3},{8,12},{9,13},{10,... | collective-permute-start | bytes 589832 | tf_op jit(solution)/shard_map/ppermute | solution.py:250
  61.9 10.9 %collective-permute-start.1 = (bf16[2,3,64,512]{3,2,1,0:T(8,128)(2,1)S(1)}, bf16[2,3,64,512]{3,2,1,0:T(8,128)(2,1)S(1)}, u32[]{:S(2)}, u32[]{:S(2)}) collective-permute-start(bf16[2,3,64,512]{3,2,1,0:T(8,128)(2,1)S(1)} %pad_maximum_fusion.4), channel_id=1, source_target_pairs={{0,2},{1,3},{2,0},{3,1},{4,6},{5,7},{6,4},{7,5},{8,10},{9,11},{10,... | collective-permute-start | bytes 1179656 | tf_op jit(solution)/shard_map/ppermute | solution.py:250
  73.6 20.0 %collective-permute-start.2 = (bf16[4,3,64,256]{3,2,1,0:T(8,128)(2,1)}, bf16[4,3,64,256]{3,2,1,0:T(8,128)(2,1)}, u32[]{:S(2)}, u32[]{:S(2)}) collective-permute-start(bf16[4,3,64,256]{3,2,1,0:T(8,128)(2,1)} %get-tuple-element.82), channel_id=1, source_target_pairs={{0,16},{1,17},{2,18},{3,19},{4,20},{5,21},{6,22},{7,23},{8,24},{9,... | collective-permute-start | bytes 1179656 | tf_op jit(solution)/shard_map/ppermute | solution.py:250
  87.0 78.5 %all-to-all-start.1 = ((bf16[16,24,2048]{2,1,0:T(8,128)(2,1)}), bf16[16,24,2048]{2,1,0:T(8,128)(2,1)S(1)}, u32[]{:S(2)}, u32[]{:S(2)}) async-start(bf16[16,24,2048]{2,1,0:T(8,128)(2,1)} %bitcast.24), calls=%async_computation.1 | async-start | bytes 3145728 | tf_op jit(solution)/shard_map/all_to_all | solution.py:253
  94.8 33.2 %collective-permute-start.3 = (bf16[8,3,64,256]{3,2,1,0:T(8,128)(2,1)S(1)}, bf16[8,3,64,256]{3,2,1,0:T(8,128)(2,1)S(1)}, u32[]{:S(2)}, u32[]{:S(2)}) collective-permute-start(bf16[8,3,64,256]{3,2,1,0:T(8,128)(2,1)S(1)} %pad_maximum_fusion.3), channel_id=1, source_target_pairs={{0,8},{1,9},{2,10},{3,11},{4,12},{5,13},{6,14},{7,15},{8,0},{9,1},... | collective-permute-start | bytes 2359304 | tf_op jit(solution)/shard_map/ppermute | solution.py:250
  130.5 18.4 %collective-permute-start.4 = (bf16[16,3,64,256]{3,2,1,0:T(8,128)(2,1)}, bf16[16,3,64,256]{3,2,1,0:T(8,128)(2,1)}, u32[]{:S(2)}, u32[]{:S(2)}) collective-permute-start(bf16[16,3,64,256]{3,2,1,0:T(8,128)(2,1)} %pad_maximum_fusion.1), channel_id=1, source_target_pairs={{0,1},{1,0},{2,3},{3,2},{4,5},{5,4},{6,7},{7,6},{8,9},{9,8},{10,11... | collective-permute-start | bytes 4718600 | tf_op jit(solution)/shard_map/ppermute | solution.py:250
  132.6 9.8 %collective-permute-start.10 = (bf16[24,2176]{1,0:T(8,128)(2,1)S(1)}, bf16[24,2176]{1,0:T(8,128)(2,1)S(1)}, u32[]{:S(2)}, u32[]{:S(2)}) collective-permute-start(bf16[24,2176]{1,0:T(8,128)(2,1)S(1)} %get-tuple-element.50), channel_id=1, source_target_pairs={{0,5},{1,4},{2,7},{3,6},{4,1},{5,0},{6,3},{7,2},{8,13},{9,12},{10,... | collective-permute-start | bytes 313352 | tf_op jit(solution)/shard_map/ppermute | solution.py:250
  135.3 7.1 %collective-permute-start.11 = (bf16[24,2176]{1,0:T(8,128)(2,1)S(1)}, bf16[24,2176]{1,0:T(8,128)(2,1)S(1)}, u32[]{:S(2)}, u32[]{:S(2)}) collective-permute-start(bf16[24,2176]{1,0:T(8,128)(2,1)S(1)} %get-tuple-element.51), channel_id=1, source_target_pairs={{0,6},{1,7},{2,4},{3,5},{4,2},{5,3},{6,0},{7,1},{8,14},{9,15},{10,... | collective-permute-start | bytes 313352 | tf_op jit(solution)/shard_map/ppermute | solution.py:250
  136.7 9.0 %collective-permute-start.12 = (bf16[24,2176]{1,0:T(8,128)(2,1)S(1)}, bf16[24,2176]{1,0:T(8,128)(2,1)S(1)}, u32[]{:S(2)}, u32[]{:S(2)}) collective-permute-start(bf16[24,2176]{1,0:T(8,128)(2,1)S(1)} %get-tuple-element.52), channel_id=1, source_target_pairs={{0,7},{1,6},{2,5},{3,4},{4,3},{5,2},{6,1},{7,0},{8,15},{9,14},{10,... | collective-permute-start | bytes 313352 | tf_op jit(solution)/shard_map/ppermute | solution.py:250
  137.6 8.2 %collective-permute-start.13 = (bf16[24,2176]{1,0:T(8,128)(2,1)S(1)}, bf16[24,2176]{1,0:T(8,128)(2,1)S(1)}, u32[]{:S(2)}, u32[]{:S(2)}) collective-permute-start(bf16[24,2176]{1,0:T(8,128)(2,1)S(1)} %get-tuple-element.53), channel_id=1, source_target_pairs={{0,8},{1,9},{2,10},{3,11},{4,12},{5,13},{6,14},{7,15},{8,0},{9,1},... | collective-permute-start | bytes 313352 | tf_op jit(solution)/shard_map/ppermute | solution.py:250
  142.4 11.5 %collective-permute-start.15 = (bf16[24,2176]{1,0:T(8,128)(2,1)S(1)}, bf16[24,2176]{1,0:T(8,128)(2,1)S(1)}, u32[]{:S(2)}, u32[]{:S(2)}) collective-permute-start(bf16[24,2176]{1,0:T(8,128)(2,1)S(1)} %get-tuple-element.55), channel_id=1, source_target_pairs={{0,10},{1,11},{2,8},{3,9},{4,14},{5,15},{6,12},{7,13},{8,2},{9,3},... | collective-permute-start | bytes 313352 | tf_op jit(solution)/shard_map/ppermute | solution.py:250
  145.8 8.8 %collective-permute-start.16 = (bf16[24,2176]{1,0:T(8,128)(2,1)S(1)}, bf16[24,2176]{1,0:T(8,128)(2,1)S(1)}, u32[]{:S(2)}, u32[]{:S(2)}) collective-permute-start(bf16[24,2176]{1,0:T(8,128)(2,1)S(1)} %get-tuple-element.56), channel_id=1, source_target_pairs={{0,11},{1,10},{2,9},{3,8},{4,15},{5,14},{6,13},{7,12},{8,3},{9,2},... | collective-permute-start | bytes 313352 | tf_op jit(solution)/shard_map/ppermute | solution.py:250
  145.8 10.5 %collective-permute-start.17 = (bf16[24,2176]{1,0:T(8,128)(2,1)S(1)}, bf16[24,2176]{1,0:T(8,128)(2,1)S(1)}, u32[]{:S(2)}, u32[]{:S(2)}) collective-permute-start(bf16[24,2176]{1,0:T(8,128)(2,1)S(1)} %get-tuple-element.57), channel_id=1, source_target_pairs={{0,12},{1,13},{2,14},{3,15},{4,8},{5,9},{6,10},{7,11},{8,4},{9,5},... | collective-permute-start | bytes 313352 | tf_op jit(solution)/shard_map/ppermute | solution.py:250
  148.1 9.2 %collective-permute-start.18 = (bf16[24,2176]{1,0:T(8,128)(2,1)S(1)}, bf16[24,2176]{1,0:T(8,128)(2,1)S(1)}, u32[]{:S(2)}, u32[]{:S(2)}) collective-permute-start(bf16[24,2176]{1,0:T(8,128)(2,1)S(1)} %get-tuple-element.58), channel_id=1, source_target_pairs={{0,13},{1,12},{2,15},{3,14},{4,9},{5,8},{6,11},{7,10},{8,5},{9,4},... | collective-permute-start | bytes 313352 | tf_op jit(solution)/shard_map/ppermute | solution.py:250
  149.0 12.1 %collective-permute-start.19 = (bf16[24,2176]{1,0:T(8,128)(2,1)S(1)}, bf16[24,2176]{1,0:T(8,128)(2,1)S(1)}, u32[]{:S(2)}, u32[]{:S(2)}) collective-permute-start(bf16[24,2176]{1,0:T(8,128)(2,1)S(1)} %get-tuple-element.59), channel_id=1, source_target_pairs={{0,14},{1,15},{2,12},{3,13},{4,10},{5,11},{6,8},{7,9},{8,6},{9,7},... | collective-permute-start | bytes 313352 | tf_op jit(solution)/shard_map/ppermute | solution.py:250
  154.0 13.4 %collective-permute-start.20 = (bf16[24,2176]{1,0:T(8,128)(2,1)S(1)}, bf16[24,2176]{1,0:T(8,128)(2,1)}, u32[]{:S(2)}, u32[]{:S(2)}) collective-permute-start(bf16[24,2176]{1,0:T(8,128)(2,1)S(1)} %get-tuple-element.60), channel_id=1, source_target_pairs={{0,15},{1,14},{2,13},{3,12},{4,11},{5,10},{6,9},{7,8},{8,7},{9,6},... | collective-permute-start | bytes 313352 | tf_op jit(solution)/shard_map/ppermute | solution.py:250
  154.6 16.2 %collective-permute-start.6 = (bf16[24,2176]{1,0:T(8,128)(2,1)S(1)}, bf16[24,2176]{1,0:T(8,128)(2,1)}, u32[]{:S(2)}, u32[]{:S(2)}) collective-permute-start(bf16[24,2176]{1,0:T(8,128)(2,1)S(1)} %get-tuple-element.46), channel_id=1, source_target_pairs={{0,1},{1,0},{2,3},{3,2},{4,5},{5,4},{6,7},{7,6},{8,9},{9,8},{10,11... | collective-permute-start | bytes 313352 | tf_op jit(solution)/shard_map/ppermute | solution.py:250
  156.3 14.5 %collective-permute-start.7 = (bf16[24,2176]{1,0:T(8,128)(2,1)S(1)}, bf16[24,2176]{1,0:T(8,128)(2,1)}, u32[]{:S(2)}, u32[]{:S(2)}) collective-permute-start(bf16[24,2176]{1,0:T(8,128)(2,1)S(1)} %get-tuple-element.47), channel_id=1, source_target_pairs={{0,2},{1,3},{2,0},{3,1},{4,6},{5,7},{6,4},{7,5},{8,10},{9,11},{10,... | collective-permute-start | bytes 313352 | tf_op jit(solution)/shard_map/ppermute | solution.py:250
  157.3 13.5 %collective-permute-start.8 = (bf16[24,2176]{1,0:T(8,128)(2,1)S(1)}, bf16[24,2176]{1,0:T(8,128)(2,1)}, u32[]{:S(2)}, u32[]{:S(2)}) collective-permute-start(bf16[24,2176]{1,0:T(8,128)(2,1)S(1)} %get-tuple-element.48), channel_id=1, source_target_pairs={{0,3},{1,2},{2,1},{3,0},{4,7},{5,6},{6,5},{7,4},{8,11},{9,10},{10,... | collective-permute-start | bytes 313352 | tf_op jit(solution)/shard_map/ppermute | solution.py:250
  161.1 9.6 %collective-permute-start.9 = (bf16[24,2176]{1,0:T(8,128)(2,1)S(1)}, bf16[24,2176]{1,0:T(8,128)(2,1)}, u32[]{:S(2)}, u32[]{:S(2)}) collective-permute-start(bf16[24,2176]{1,0:T(8,128)(2,1)S(1)} %get-tuple-element.49), channel_id=1, source_target_pairs={{0,4},{1,5},{2,6},{3,7},{4,0},{5,1},{6,2},{7,3},{8,12},{9,13},{10,... | collective-permute-start | bytes 313352 | tf_op jit(solution)/shard_map/ppermute | solution.py:250
  167.4 44.9 %collective-permute-start.38 = (bf16[128,2048]{1,0:T(8,128)(2,1)S(1)}, bf16[128,2048]{1,0:T(8,128)(2,1)S(1)}, u32[]{:S(2)}, u32[]{:S(2)}) collective-permute-start(bf16[128,2048]{1,0:T(8,128)(2,1)S(1)} %shard_map.108), channel_id=1, source_target_pairs={{0,16},{1,17},{2,18},{3,19},{4,20},{5,21},{6,22},{7,23},{8,24},{9,... | collective-permute-start | bytes 1572872 | tf_op jit(solution)/shard_map/ppermute | solution.py:250
  183.6 7.4 %collective-permute-start.25 = (bf16[24,2048]{1,0:T(8,128)(2,1)}, bf16[24,2048]{1,0:T(8,128)(2,1)S(1)}, u32[]{:S(2)}, u32[]{:S(2)}) collective-permute-start(bf16[24,2048]{1,0:T(8,128)(2,1)} %get-tuple-element.66), channel_id=1, source_target_pairs={{0,5},{1,4},{2,7},{3,6},{4,1},{5,0},{6,3},{7,2},{8,13},{9,12},{10,... | collective-permute-start | bytes 294920 | tf_op jit(solution)/shard_map/ppermute | solution.py:250
  193.1 7.0 %collective-permute-start.30 = (bf16[24,2048]{1,0:T(8,128)(2,1)}, bf16[24,2048]{1,0:T(8,128)(2,1)S(1)}, u32[]{:S(2)}, u32[]{:S(2)}) collective-permute-start(bf16[24,2048]{1,0:T(8,128)(2,1)} %get-tuple-element.71), channel_id=1, source_target_pairs={{0,10},{1,11},{2,8},{3,9},{4,14},{5,15},{6,12},{7,13},{8,2},{9,3},... | collective-permute-start | bytes 294920 | tf_op jit(solution)/shard_map/ppermute | solution.py:250
  194.7 8.0 %collective-permute-start.31 = (bf16[24,2048]{1,0:T(8,128)(2,1)}, bf16[24,2048]{1,0:T(8,128)(2,1)S(1)}, u32[]{:S(2)}, u32[]{:S(2)}) collective-permute-start(bf16[24,2048]{1,0:T(8,128)(2,1)} %get-tuple-element.72), channel_id=1, source_target_pairs={{0,11},{1,10},{2,9},{3,8},{4,15},{5,14},{6,13},{7,12},{8,3},{9,2},... | collective-permute-start | bytes 294920 | tf_op jit(solution)/shard_map/ppermute | solution.py:250
  196.5 8.0 %collective-permute-start.32 = (bf16[24,2048]{1,0:T(8,128)(2,1)}, bf16[24,2048]{1,0:T(8,128)(2,1)S(1)}, u32[]{:S(2)}, u32[]{:S(2)}) collective-permute-start(bf16[24,2048]{1,0:T(8,128)(2,1)} %get-tuple-element.73), channel_id=1, source_target_pairs={{0,12},{1,13},{2,14},{3,15},{4,8},{5,9},{6,10},{7,11},{8,4},{9,5},... | collective-permute-start | bytes 294920 | tf_op jit(solution)/shard_map/ppermute | solution.py:250
  197.6 8.3 %collective-permute-start.33 = (bf16[24,2048]{1,0:T(8,128)(2,1)}, bf16[24,2048]{1,0:T(8,128)(2,1)S(1)}, u32[]{:S(2)}, u32[]{:S(2)}) collective-permute-start(bf16[24,2048]{1,0:T(8,128)(2,1)} %get-tuple-element.74), channel_id=1, source_target_pairs={{0,13},{1,12},{2,15},{3,14},{4,9},{5,8},{6,11},{7,10},{8,5},{9,4},... | collective-permute-start | bytes 294920 | tf_op jit(solution)/shard_map/ppermute | solution.py:250
  200.1 8.3 %collective-permute-start.34 = (bf16[24,2048]{1,0:T(8,128)(2,1)}, bf16[24,2048]{1,0:T(8,128)(2,1)S(1)}, u32[]{:S(2)}, u32[]{:S(2)}) collective-permute-start(bf16[24,2048]{1,0:T(8,128)(2,1)} %get-tuple-element.75), channel_id=1, source_target_pairs={{0,14},{1,15},{2,12},{3,13},{4,10},{5,11},{6,8},{7,9},{8,6},{9,7},... | collective-permute-start | bytes 294920 | tf_op jit(solution)/shard_map/ppermute | solution.py:250
  202.7 7.9 %collective-permute-start.35 = (bf16[24,2048]{1,0:T(8,128)(2,1)}, bf16[24,2048]{1,0:T(8,128)(2,1)S(1)}, u32[]{:S(2)}, u32[]{:S(2)}) collective-permute-start(bf16[24,2048]{1,0:T(8,128)(2,1)} %get-tuple-element.76), channel_id=1, source_target_pairs={{0,15},{1,14},{2,13},{3,12},{4,11},{5,10},{6,9},{7,8},{8,7},{9,6},... | collective-permute-start | bytes 294920 | tf_op jit(solution)/shard_map/ppermute | solution.py:250
  (34 other events, 286.1 us)

commit v2 on v1

--- a/solution.py
+++ b/solution.py
@@ -61,11 +61,13 @@
     pick, labels, mix = routes(place_ref, ids_ref, weights_ref, **sizes)
     mix_ref[...] = mix
     width = x_ref.shape[1]
-    cap = sizes["cap"]
     sent = jnp.dot(pick, x_ref[...], preferred_element_type=F32).astype(BF16)
-    for slot, out_ref in enumerate(out_refs):
-        out_ref[:, :width] = sent[slot * cap : (slot + 1) * cap]
-        out_ref[:, width:] = labels[slot * cap : (slot + 1) * cap]
+    start = 0
+    for out_ref in out_refs:
+        stop = start + out_ref.shape[0]
+        out_ref[:, :width] = sent[start:stop]
+        out_ref[:, width:] = labels[start:stop]
+        start = stop
 
 
 def route_kernel(place_ref, ids_ref, weights_ref, pick_ref, label_ref, mix_ref, **sizes):
@@ -82,11 +84,25 @@
     out_ref[:, width:] = label_ref[...]
 
 
-def join(refs, rows_ref):
+def join(refs, rows_ref, takes=None):
     start = 0
-    for ref in refs:
-        rows_ref[start : start + ref.shape[0], :] = ref[...]
-        start += ref.shape[0]
+    for ref, take in zip(refs, takes or [ref.shape[0] for ref in refs]):
+        rows_ref[start : start + take, :] = ref[:take]
+        start += take
+
+
+def swap_kernel(*refs):
+    *in_refs, out_ref = refs
+    cap = in_refs[0].shape[0] // 2
+    for i, ref in enumerate(in_refs):
+        out_ref[i * cap : (i + 1) * cap, :] = ref[cap:]
+
+
+def merge_kernel(kept_ref, swapped_ref, *out_refs):
+    cap = out_refs[0].shape[0] // 2
+    for i, ref in enumerate(out_refs):
+        ref[:cap] = kept_ref[i * cap : (i + 1) * cap, :]
+        ref[cap:] = swapped_ref[i * cap : (i + 1) * cap, :]
 
 
 def combined(mix_ref, back_ref):
@@ -109,9 +125,9 @@
     out_ref[...] = (own_ref[...] + other_ref[...].astype(F32)).astype(BF16)
 
 
-def expert_kernel(gate_ref, up_ref, down_ref, *refs, pieces, cuts, outs):
-    in_refs, out_refs = refs[:pieces], refs[pieces : 2 * pieces]
-    gate_buf, up_buf, down_buf, hidden_ref, sems, *rest = refs[2 * pieces :]
+def expert_kernel(gate_ref, up_ref, down_ref, *refs, takes, results, cuts, outs):
+    in_refs, out_refs = refs[: len(takes)], refs[len(takes) : len(takes) + results]
+    gate_buf, up_buf, down_buf, hidden_ref, sems, *rest = refs[len(takes) + results :]
     rows_ref = rest[0] if rest else in_refs[0]
     experts, width, hidden = gate_ref.shape
     block = hidden // cuts
@@ -133,7 +149,7 @@
         copy.start()
         seconds.append(copy)
     if rest:
-        join(in_refs, rows_ref)
+        join(in_refs, rows_ref, takes)
     for i, (e, _) in enumerate(parts):
         for copy in firsts[i]:
             copy.wait()
@@ -155,12 +171,12 @@
             start = stop
 
 
-def run_experts(rows, w_gate, w_up, w_down):
+def run_experts(rows, takes, results, w_gate, w_up, w_down):
     experts, width, hidden = w_gate.shape
     cuts, outs = 2, 2
     steps = experts * cuts
     block, piece = hidden // cuts, width // outs
-    count = sum(part.shape[0] for part in rows)
+    count = sum(takes)
     scratch = [
         pltpu.VMEM((steps, width, block), BF16),
         pltpu.VMEM((steps, width, block), BF16),
@@ -171,10 +187,12 @@
     if len(rows) > 1:
         scratch.append(pltpu.VMEM((count, rows[0].shape[1]), BF16))
     return pl.pallas_call(
-        functools.partial(expert_kernel, pieces=len(rows), cuts=cuts, outs=outs),
+        functools.partial(
+            expert_kernel, takes=tuple(takes), results=len(results), cuts=cuts, outs=outs
+        ),
         in_specs=[pl.BlockSpec(memory_space=pltpu.HBM)] * 3 + [VMEM] * len(rows),
-        out_specs=[VMEM] * len(rows),
-        out_shape=[jax.ShapeDtypeStruct((part.shape[0], width), BF16) for part in rows],
+        out_specs=[VMEM] * len(results),
+        out_shape=[jax.ShapeDtypeStruct((part, width), BF16) for part in results],
         scratch_shapes=scratch,
         cost_estimate=pl.CostEstimate(
             flops=6 * count * experts * width * hidden,
@@ -281,27 +299,39 @@
     ids, weights = expert_ids.T, gate_weights.T
     ids_other = exchange(ids, half)
     weights_other = exchange(weights, half)
-    piece = jax.ShapeDtypeStruct((cap, width + LANES), BF16)
+    chips = half // 2
+    piece = jax.ShapeDtypeStruct((2 * cap, width + LANES), BF16)
     normed = call(
         norm_kernel, dense, (tokens, norm_gain.reshape(1, width)),
         scalars=0, flops=8 * count * width,
     )
     normed_other = exchange(normed, half)
     mix, *outgoing = call(
-        functools.partial(front_kernel, **sizes), [plan[2]] + [piece] * half,
+        functools.partial(front_kernel, **sizes), [plan[2]] + [piece] * chips,
         (place, ids, weights, normed), flops=work + few,
     )
-    incoming = [outgoing[0]] + [exchange(outgoing[r], r) for r in range(1, half)]
+    incoming = [outgoing[0]] + [exchange(outgoing[m], 2 * m) for m in range(1, chips)]
+    crossing = call(
+        swap_kernel, jax.ShapeDtypeStruct((rows // 2, width + LANES), BF16), incoming,
+        scalars=0,
+    )
+    crossed = exchange(crossing, 1)
     pick, label, mix_other = call(
         functools.partial(route_kernel, **sizes), plan,
         (place_other, ids_other, weights_other), flops=few,
     )
     outgoing_other = call(gather_kernel, sent, (pick, label, normed_other), scalars=0, flops=work)
     incoming_other = within(outgoing_other)
-    results = run_experts(incoming, expert_gate, expert_up, expert_down)
-    (results_other,) = run_experts([incoming_other], expert_gate, expert_up, expert_down)
+    experts = (expert_gate, expert_up, expert_down)
+    kept, crossing = run_experts(
+        incoming + [crossed], [cap] * chips + [rows // 2], [rows // 2] * 2, *experts
+    )
+    (results_other,) = run_experts([incoming_other], [rows], [rows], *experts)
     back_other = within(results_other)
-    back = [results[0]] + [exchange(results[r], r) for r in range(1, half)]
+    crossed = exchange(crossing, 1)
+    piece = jax.ShapeDtypeStruct((2 * cap, width), BF16)
+    results = call(merge_kernel, [piece] * chips, (kept, crossed), scalars=0)
+    back = [results[0]] + [exchange(results[m], 2 * m) for m in range(1, chips)]
 
     block = shared_gate.shape[0]
     full = pltpu.VMEM((devices * block, cut), BF16)

time: 214 us -> 214 us (level)
  starting transfers between devices: 64.1 us -> 49.7 us
  waiting for transfers between devices: 106 us -> 120 us
    ppermute x39 -> x25, starting transfers between devices: 55.5 us -> 41.1 us  [exchange(): return lax.ppermute(array, 'ep', [(i, i ^ bit) for i in range(devices)])]
    ppermute x39 -> x25, waiting for transfers between devices: 106 us -> 120 us  [exchange(): return lax.ppermute(array, 'ep', [(i, i ^ bit) for i in range(devices)])]
    unnamed x50 -> x56, local copies, waits for them, and re-layouts: 6.83 us -> 7.3 us
    pallas_call x8 -> x10, Pallas kernels: 8.29 us -> 8.47 us  [call(): pl.pallas_call(kernel, in_specs=[SMEM] * scalars + [VMEM] * (len(args) -...]
  transfers between devices with their start and end apart: 41 -> 27, of which waited for: 17 -> 14; matrix products, arithmetic and copies ran while one was open for 3% -> 3% of each run, Pallas kernels for 12% -> 12%
where the time goes in v2:
time: 214 us; the launch traced here: 213 us
  waiting for transfers between devices  120 us (56%)
  starting transfers between devices  49.7 us (23%)
  Pallas kernels  29.3 us (14%)
  local copies, waits for them, and re-layouts  7.3 us (3%)
  other arithmetic  6.45 us (3%)
    ppermute x25, waiting for transfers between devices, exchange(): return lax.ppermute(array, 'ep', [(i, i ^ bit) for i in range(devices)])  120 us
    ppermute x25, starting transfers between devices, exchange(): return lax.ppermute(array, 'ep', [(i, i ^ bit) for i in range(devices)])  41.1 us
    pallas_call x2, Pallas kernels, run_experts(): pl.pallas_call(functools.partial(expert_kernel, takes=tuple(takes), resul...  20.8 us
    all_to_all x2, starting transfers between devices, within(): lax.all_to_all(array, 'ep', 0, 0, axis_index_groups=groups, tiled=True)  8.58 us
    pallas_call x10, Pallas kernels, call(): pl.pallas_call(kernel, in_specs=[SMEM] * scalars + [VMEM] * (len(args) -...  8.47 us
    unnamed x56, local copies, waits for them, and re-layouts  7.3 us
    concatenate x5, other arithmetic, per_device(): parts = jnp.concatenate([mine, exchange(theirs, bit)], axis=0)  5.48 us
  transfers between devices with their start and end apart: 27, of which 14 were waited for; matrix products, arithmetic and copies ran while one was open for 3% of the time, Pallas kernels for 12%

profile of v2, /device:TPU:0, one launch (start us, length us, event | category | flops | bytes accessed | tf_op | source)
XLA Modules:
  0.0 213.2 jit_solution(16910346640217070029)
XLA Ops:
  2.0 4.1 %collective-permute-start.5 = (bf16[128,2048]{1,0:T(8,128)(2,1)S(1)}, bf16[128,2048]{1,0:T(8,128)(2,1)S(1)}, u32[]{:S(2)}, u32[]{:S(2)}) collective-permute-start(bf16[128,2048]{1,0:T(8,128)(2,1)S(1)} %shard_map.100.x_ref.own_ref), channel_id=1, source_target_pairs={{0,16},{1,17},{2,18},{3,19},{4,20},{5,21},{6,22},{7,23},{8,24},{9,... | collective-permute-start | bytes 1572872 | tf_op jit(solution)/shard_map/ppermute | solution.py:268
  6.2 2.8 %collective-permute-start.23 = (f32[4,128]{1,0:T(4,128)}, f32[4,128]{1,0:T(4,128)S(1)}, u32[]{:S(2)}, u32[]{:S(2)}) collective-permute-start(f32[4,128]{1,0:T(4,128)} %bitcast.22), channel_id=1, source_target_pairs={{0,16},{1,17},{2,18},{3,19},{4,20},{5,21},{6,22},{7,23},{8,24},{9,... | collective-permute-start | bytes 6152 | tf_op jit(solution)/shard_map/ppermute | solution.py:268
  9.1 20.3 %collective-permute-done.22.ids_ref = s32[4,128]{1,0:T(4,128)S(1)} collective-permute-done((s32[4,128]{1,0:T(4,128)}, s32[4,128]{1,0:T(4,128)S(1)}, u32[]{:S(2)}, u32[]{:S(2)}) %collective-permute-start.22) | collective-permute-done | bytes 2080 | tf_op jit(solution)/shard_map/ppermute | solution.py:268
  31.1 1.8 shard_map.108
  32.9 4.5 %all-to-all-start = ((bf16[16,24,2176]{2,1,0:T(8,128)(2,1)}), bf16[16,24,2176]{2,1,0:T(8,128)(2,1)}, u32[]{:S(2)}, u32[]{:S(2)}) async-start(bf16[16,24,2176]{2,1,0:T(8,128)(2,1)} %bitcast.12), calls=%async_computation | async-start | bytes 3342336 | tf_op jit(solution)/shard_map/all_to_all | solution.py:271
  37.5 1.8 collective-permute-start
  39.4 23.2 %collective-permute-done = bf16[1,3,64,512]{3,2,1,0:T(8,128)(2,1)S(1)} collective-permute-done((bf16[1,3,64,512]{3,2,1,0:T(8,128)(2,1)S(1)}, bf16[1,3,64,512]{3,2,1,0:T(8,128)(2,1)S(1)}, u32[]{:S(2)}, u32[]{:S(2)}) %collective-permute-start) | collective-permute-done | bytes 196640 | tf_op jit(solution)/shard_map/ppermute | solution.py:268
  64.1 9.3 %collective-permute-done.1 = bf16[2,3,64,512]{3,2,1,0:T(8,128)(2,1)S(1)} collective-permute-done((bf16[2,3,64,512]{3,2,1,0:T(8,128)(2,1)S(1)}, bf16[2,3,64,512]{3,2,1,0:T(8,128)(2,1)S(1)}, u32[]{:S(2)}, u32[]{:S(2)}) %collective-permute-start.1) | collective-permute-done | bytes 393248 | tf_op jit(solution)/shard_map/ppermute | solution.py:268
  74.3 3.1 %collective-permute-start.2 = (bf16[4,3,64,256]{3,2,1,0:T(8,128)(2,1)}, bf16[4,3,64,256]{3,2,1,0:T(8,128)(2,1)S(1)}, u32[]{:S(2)}, u32[]{:S(2)}) collective-permute-start(bf16[4,3,64,256]{3,2,1,0:T(8,128)(2,1)} %get-tuple-element.54), channel_id=1, source_target_pairs={{0,16},{1,17},{2,18},{3,19},{4,20},{5,21},{6,22},{7,23},{8,24},{9,... | collective-permute-start | bytes 1179656 | tf_op jit(solution)/shard_map/ppermute | solution.py:268
  77.4 10.2 %shard_map.109 = bf16[384,2048]{1,0:T(8,128)(2,1)} custom-call(bf16[2,2048,512]{2,1,0:T(8,128)(2,1)} %gate_ref.3, bf16[2,2048,512]{2,1,0:T(8,128)(2,1)} %up_ref.3, bf16[1024,2048]{1,0:T(8,128)(2,1)} %bitcast.28, bf16[384,2176]{1,0:T(8,128)(2,1)} %bitcast.13.refs_0_), custom_call_target="tpu_custom_call" | custom-call | flops 4831838208 | bytes 15728640 | tf_op jit(solution)/shard_map/pallas_call | solution.py:189
  87.7 4.0 %all-to-all-start.1 = ((bf16[16,24,2048]{2,1,0:T(8,128)(2,1)}), bf16[16,24,2048]{2,1,0:T(8,128)(2,1)S(1)}, u32[]{:S(2)}, u32[]{:S(2)}) async-start(bf16[16,24,2048]{2,1,0:T(8,128)(2,1)} %bitcast.24), calls=%async_computation.1 | async-start | bytes 3145728 | tf_op jit(solution)/shard_map/all_to_all | solution.py:271
  91.8 2.5 %collective-permute-done.2 = bf16[4,3,64,256]{3,2,1,0:T(8,128)(2,1)S(1)} collective-permute-done((bf16[4,3,64,256]{3,2,1,0:T(8,128)(2,1)}, bf16[4,3,64,256]{3,2,1,0:T(8,128)(2,1)S(1)}, u32[]{:S(2)}, u32[]{:S(2)}) %collective-permute-start.2) | collective-permute-done | bytes 393248 | tf_op jit(solution)/shard_map/ppermute | solution.py:268
  98.2 2.6 %collective-permute-start.10 = (bf16[48,2176]{1,0:T(8,128)(2,1)S(1)}, bf16[48,2176]{1,0:T(8,128)(2,1)S(1)}, u32[]{:S(2)}, u32[]{:S(2)}) collective-permute-start(bf16[48,2176]{1,0:T(8,128)(2,1)S(1)} %get-tuple-element.36), channel_id=1, source_target_pairs={{0,10},{1,11},{2,8},{3,9},{4,14},{5,15},{6,12},{7,13},{8,2},{9,3},... | collective-permute-start | bytes 626696 | tf_op jit(solution)/shard_map/ppermute | solution.py:268
  101.6 1.7 collective-permute-start.12
  103.2 2.0 collective-permute-start.6
  105.2 30.2 %collective-permute-done.10.refs_5_ = bf16[48,2176]{1,0:T(8,128)(2,1)S(1)} collective-permute-done((bf16[48,2176]{1,0:T(8,128)(2,1)S(1)}, bf16[48,2176]{1,0:T(8,128)(2,1)S(1)}, u32[]{:S(2)}, u32[]{:S(2)}) %collective-permute-start.10) | collective-permute-done | bytes 208928 | tf_op jit(solution)/shard_map/ppermute | solution.py:268
  136.8 3.6 %collective-permute-done.11.refs_6_ = bf16[48,2176]{1,0:T(8,128)(2,1)S(1)} collective-permute-done((bf16[48,2176]{1,0:T(8,128)(2,1)S(1)}, bf16[48,2176]{1,0:T(8,128)(2,1)S(1)}, u32[]{:S(2)}, u32[]{:S(2)}) %collective-permute-start.11) | collective-permute-done | bytes 208928 | tf_op jit(solution)/shard_map/ppermute | solution.py:268
  140.3 1.9 collective-permute-start.8
  142.2 2.5 %collective-permute-done.12.refs_7_ = bf16[48,2176]{1,0:T(8,128)(2,1)S(1)} collective-permute-done((bf16[48,2176]{1,0:T(8,128)(2,1)S(1)}, bf16[48,2176]{1,0:T(8,128)(2,1)S(1)}, u32[]{:S(2)}, u32[]{:S(2)}) %collective-permute-start.12) | collective-permute-done | bytes 208928 | tf_op jit(solution)/shard_map/ppermute | solution.py:268
  145.2 7.9 %collective-permute-done.7.refs_2_ = bf16[48,2176]{1,0:T(8,128)(2,1)S(1)} collective-permute-done((bf16[48,2176]{1,0:T(8,128)(2,1)S(1)}, bf16[48,2176]{1,0:T(8,128)(2,1)S(1)}, u32[]{:S(2)}, u32[]{:S(2)}) %collective-permute-start.7) | collective-permute-done | bytes 208928 | tf_op jit(solution)/shard_map/ppermute | solution.py:268
  153.3 2.5 %pad_maximum_fusion.1 = bf16[16,3,64,256]{3,2,1,0:T(8,128)(2,1)} fusion(bf16[8,3,64,256]{3,2,1,0:T(8,128)(2,1)} %collective-permute-done.3, bf16[4,3,64,256]{3,2,1,0:T(8,128)(2,1)S(1)} %collective-permute-done.2, bf16[4,3,64,256]{3,2,1,0:T(8,128)(2,1)S(1)} %copy-done.22), kind=kLoop, calls=%fused_computation.1 | loop fusion | flops 1572864 | bytes 3145728 | tf_op jit(solution)/shard_map/concatenate | solution.py:296
  156.4 10.6 %shard_map.104 = (bf16[192,2048]{1,0:T(8,128)(2,1)}, bf16[192,2048]{1,0:T(8,128)(2,1)}) custom-call(bf16[2,2048,512]{2,1,0:T(8,128)(2,1)} %gate_ref.3, bf16[2,2048,512]{2,1,0:T(8,128)(2,1)} %up_ref.3, bf16[1024,2048]{1,0:T(8,128)(2,1)} %bitcast.29, bf16[48,2176]{1,0:T(8,128)(2,1)} %copy-done.6, bf16[48,2176]{1,0:T(8,128)(2,1)} %copy-done.10, ...), custom_call_target="tpu_custom_call" | custom-call | flops 4831838208 | bytes 15728640 | tf_op jit(solution)/shard_map/pallas_call | solution.py:189
  167.1 1.9 pad_maximum_fusion.parts_ref
  169.0 1.7 shard_map.102
  176.0 2.3 %collective-permute-start.15 = (bf16[48,2048]{1,0:T(8,128)(2,1)S(1)}, bf16[48,2048]{1,0:T(8,128)(2,1)S(1)}, u32[]{:S(2)}, u32[]{:S(2)}) collective-permute-start(bf16[48,2048]{1,0:T(8,128)(2,1)S(1)} %get-tuple-element.42), channel_id=1, source_target_pairs={{0,2},{1,3},{2,0},{3,1},{4,6},{5,7},{6,4},{7,5},{8,10},{9,11},{10,... | collective-permute-start | bytes 589832 | tf_op jit(solution)/shard_map/ppermute | solution.py:268
  178.3 1.7 collective-permute-start.16
  181.4 1.7 collective-permute-start.18
  184.0 3.4 %collective-permute-start.19 = (bf16[48,2048]{1,0:T(8,128)(2,1)S(1)}, bf16[48,2048]{1,0:T(8,128)(2,1)S(1)}, u32[]{:S(2)}, u32[]{:S(2)}) collective-permute-start(bf16[48,2048]{1,0:T(8,128)(2,1)S(1)} %get-tuple-element.46), channel_id=1, source_target_pairs={{0,10},{1,11},{2,8},{3,9},{4,14},{5,15},{6,12},{7,13},{8,2},{9,3},... | collective-permute-start | bytes 589832 | tf_op jit(solution)/shard_map/ppermute | solution.py:268
  188.7 4.4 %collective-permute-start.20 = (bf16[48,2048]{1,0:T(8,128)(2,1)S(1)}, bf16[48,2048]{1,0:T(8,128)(2,1)S(1)}, u32[]{:S(2)}, u32[]{:S(2)}) collective-permute-start(bf16[48,2048]{1,0:T(8,128)(2,1)S(1)} %get-tuple-element.47), channel_id=1, source_target_pairs={{0,12},{1,13},{2,14},{3,15},{4,8},{5,9},{6,10},{7,11},{8,4},{9,5},... | collective-permute-start | bytes 589832 | tf_op jit(solution)/shard_map/ppermute | solution.py:268
  194.5 9.6 %collective-permute-done.19.refs_5_ = bf16[48,2048]{1,0:T(8,128)(2,1)S(1)} collective-permute-done((bf16[48,2048]{1,0:T(8,128)(2,1)S(1)}, bf16[48,2048]{1,0:T(8,128)(2,1)S(1)}, u32[]{:S(2)}, u32[]{:S(2)}) %collective-permute-start.19) | collective-permute-done | bytes 196640 | tf_op jit(solution)/shard_map/ppermute | solution.py:268
  204.2 4.0 %collective-permute-done.20.refs_6_ = bf16[48,2048]{1,0:T(8,128)(2,1)S(1)} collective-permute-done((bf16[48,2048]{1,0:T(8,128)(2,1)S(1)}, bf16[48,2048]{1,0:T(8,128)(2,1)S(1)}, u32[]{:S(2)}, u32[]{:S(2)}) %collective-permute-start.20) | collective-permute-done | bytes 196640 | tf_op jit(solution)/shard_map/ppermute | solution.py:268
  208.2 3.4 %collective-permute-done.21.refs_7_ = bf16[48,2048]{1,0:T(8,128)(2,1)S(1)} collective-permute-done((bf16[48,2048]{1,0:T(8,128)(2,1)S(1)}, bf16[48,2048]{1,0:T(8,128)(2,1)S(1)}, u32[]{:S(2)}, u32[]{:S(2)}) %collective-permute-start.21) | collective-permute-done | bytes 196640 | tf_op jit(solution)/shard_map/ppermute | solution.py:268
  (99 shorter events, 25.5 us)
Async XLA Ops:
  2.0 29.2 %collective-permute-start.5 = (bf16[128,2048]{1,0:T(8,128)(2,1)S(1)}, bf16[128,2048]{1,0:T(8,128)(2,1)S(1)}, u32[]{:S(2)}, u32[]{:S(2)}) collective-permute-start(bf16[128,2048]{1,0:T(8,128)(2,1)S(1)} %shard_map.100.x_ref.own_ref), channel_id=1, source_target_pairs={{0,16},{1,17},{2,18},{3,19},{4,20},{5,21},{6,22},{7,23},{8,24},{9,... | collective-permute-start | bytes 1572872 | tf_op jit(solution)/shard_map/ppermute | solution.py:268
  6.1 23.3 %collective-permute-start.22 = (s32[4,128]{1,0:T(4,128)}, s32[4,128]{1,0:T(4,128)S(1)}, u32[]{:S(2)}, u32[]{:S(2)}) collective-permute-start(s32[4,128]{1,0:T(4,128)} %bitcast.20), channel_id=1, source_target_pairs={{0,16},{1,17},{2,18},{3,19},{4,20},{5,21},{6,22},{7,23},{8,24},{9,... | collective-permute-start | bytes 6152 | tf_op jit(solution)/shard_map/ppermute | solution.py:268
  6.2 23.3 %collective-permute-start.23 = (f32[4,128]{1,0:T(4,128)}, f32[4,128]{1,0:T(4,128)S(1)}, u32[]{:S(2)}, u32[]{:S(2)}) collective-permute-start(f32[4,128]{1,0:T(4,128)} %bitcast.22), channel_id=1, source_target_pairs={{0,16},{1,17},{2,18},{3,19},{4,20},{5,21},{6,22},{7,23},{8,24},{9,... | collective-permute-start | bytes 6152 | tf_op jit(solution)/shard_map/ppermute | solution.py:268
  32.9 44.5 %all-to-all-start = ((bf16[16,24,2176]{2,1,0:T(8,128)(2,1)}), bf16[16,24,2176]{2,1,0:T(8,128)(2,1)}, u32[]{:S(2)}, u32[]{:S(2)}) async-start(bf16[16,24,2176]{2,1,0:T(8,128)(2,1)} %bitcast.12), calls=%async_computation | async-start | bytes 3342336 | tf_op jit(solution)/shard_map/all_to_all | solution.py:271
  37.5 25.0 %collective-permute-start = (bf16[1,3,64,512]{3,2,1,0:T(8,128)(2,1)S(1)}, bf16[1,3,64,512]{3,2,1,0:T(8,128)(2,1)S(1)}, u32[]{:S(2)}, u32[]{:S(2)}) collective-permute-start(bf16[1,3,64,512]{3,2,1,0:T(8,128)(2,1)S(1)} %maximum_bitcast_fusion), channel_id=1, source_target_pairs={{0,4},{1,5},{2,6},{3,7},{4,0},{5,1},{6,2},{7,3},{8,12},{9,13},{10,... | collective-permute-start | bytes 589832 | tf_op jit(solution)/shard_map/ppermute | solution.py:268
  62.6 10.9 %collective-permute-start.1 = (bf16[2,3,64,512]{3,2,1,0:T(8,128)(2,1)S(1)}, bf16[2,3,64,512]{3,2,1,0:T(8,128)(2,1)S(1)}, u32[]{:S(2)}, u32[]{:S(2)}) collective-permute-start(bf16[2,3,64,512]{3,2,1,0:T(8,128)(2,1)S(1)} %pad_maximum_fusion.4), channel_id=1, source_target_pairs={{0,2},{1,3},{2,0},{3,1},{4,6},{5,7},{6,4},{7,5},{8,10},{9,11},{10,... | collective-permute-start | bytes 1179656 | tf_op jit(solution)/shard_map/ppermute | solution.py:268
  74.3 19.9 %collective-permute-start.2 = (bf16[4,3,64,256]{3,2,1,0:T(8,128)(2,1)}, bf16[4,3,64,256]{3,2,1,0:T(8,128)(2,1)S(1)}, u32[]{:S(2)}, u32[]{:S(2)}) collective-permute-start(bf16[4,3,64,256]{3,2,1,0:T(8,128)(2,1)} %get-tuple-element.54), channel_id=1, source_target_pairs={{0,16},{1,17},{2,18},{3,19},{4,20},{5,21},{6,22},{7,23},{8,24},{9,... | collective-permute-start | bytes 1179656 | tf_op jit(solution)/shard_map/ppermute | solution.py:268
  87.7 84.9 %all-to-all-start.1 = ((bf16[16,24,2048]{2,1,0:T(8,128)(2,1)}), bf16[16,24,2048]{2,1,0:T(8,128)(2,1)S(1)}, u32[]{:S(2)}, u32[]{:S(2)}) async-start(bf16[16,24,2048]{2,1,0:T(8,128)(2,1)} %bitcast.24), calls=%async_computation.1 | async-start | bytes 3145728 | tf_op jit(solution)/shard_map/all_to_all | solution.py:271
  94.3 59.0 %copy-start.24 = (bf16[4,3,64,256]{3,2,1,0:T(8,128)(2,1)}, bf16[4,3,64,256]{3,2,1,0:T(8,128)(2,1)S(1)}, u32[]{:S(2)}) copy-start(bf16[4,3,64,256]{3,2,1,0:T(8,128)(2,1)S(1)} %collective-permute-done.2) | copy-start | bytes 1179652
  95.3 58.0 %collective-permute-start.3 = (bf16[8,3,64,256]{3,2,1,0:T(8,128)(2,1)}, bf16[8,3,64,256]{3,2,1,0:T(8,128)(2,1)}, u32[]{:S(2)}, u32[]{:S(2)}) collective-permute-start(bf16[8,3,64,256]{3,2,1,0:T(8,128)(2,1)} %pad_maximum_fusion.3), channel_id=1, source_target_pairs={{0,8},{1,9},{2,10},{3,11},{4,12},{5,13},{6,14},{7,15},{8,0},{9,1},... | collective-permute-start | bytes 2359304 | tf_op jit(solution)/shard_map/ppermute | solution.py:268
  96.2 57.2 %copy-start.22 = (bf16[4,3,64,256]{3,2,1,0:T(8,128)(2,1)S(1)}, bf16[4,3,64,256]{3,2,1,0:T(8,128)(2,1)}, u32[]{:S(2)}) copy-start(bf16[4,3,64,256]{3,2,1,0:T(8,128)(2,1)} %copy-done.21) | copy-start | bytes 1179652
  98.2 57.6 %copy-start.6 = (bf16[48,2176]{1,0:T(8,128)(2,1)}, bf16[48,2176]{1,0:T(8,128)(2,1)S(1)}, u32[]{:S(2)}) copy-start(bf16[48,2176]{1,0:T(8,128)(2,1)S(1)} %get-tuple-element.31.refs_0_) | copy-start | bytes 626692
  98.2 37.2 %collective-permute-start.10 = (bf16[48,2176]{1,0:T(8,128)(2,1)S(1)}, bf16[48,2176]{1,0:T(8,128)(2,1)S(1)}, u32[]{:S(2)}, u32[]{:S(2)}) collective-permute-start(bf16[48,2176]{1,0:T(8,128)(2,1)S(1)} %get-tuple-element.36), channel_id=1, source_target_pairs={{0,10},{1,11},{2,8},{3,9},{4,14},{5,15},{6,12},{7,13},{8,2},{9,3},... | collective-permute-start | bytes 626696 | tf_op jit(solution)/shard_map/ppermute | solution.py:268
  100.9 39.5 %collective-permute-start.11 = (bf16[48,2176]{1,0:T(8,128)(2,1)S(1)}, bf16[48,2176]{1,0:T(8,128)(2,1)S(1)}, u32[]{:S(2)}, u32[]{:S(2)}) collective-permute-start(bf16[48,2176]{1,0:T(8,128)(2,1)S(1)} %get-tuple-element.37), channel_id=1, source_target_pairs={{0,12},{1,13},{2,14},{3,15},{4,8},{5,9},{6,10},{7,11},{8,4},{9,5},... | collective-permute-start | bytes 626696 | tf_op jit(solution)/shard_map/ppermute | solution.py:268
  101.6 43.2 %collective-permute-start.12 = (bf16[48,2176]{1,0:T(8,128)(2,1)S(1)}, bf16[48,2176]{1,0:T(8,128)(2,1)S(1)}, u32[]{:S(2)}, u32[]{:S(2)}) collective-permute-start(bf16[48,2176]{1,0:T(8,128)(2,1)S(1)} %get-tuple-element.38), channel_id=1, source_target_pairs={{0,14},{1,15},{2,12},{3,13},{4,10},{5,11},{6,8},{7,9},{8,6},{9,7},... | collective-permute-start | bytes 626696 | tf_op jit(solution)/shard_map/ppermute | solution.py:268
  103.2 42.0 %collective-permute-start.6 = (bf16[48,2176]{1,0:T(8,128)(2,1)S(1)}, bf16[48,2176]{1,0:T(8,128)(2,1)S(1)}, u32[]{:S(2)}, u32[]{:S(2)}) collective-permute-start(bf16[48,2176]{1,0:T(8,128)(2,1)S(1)} %get-tuple-element.32), channel_id=1, source_target_pairs={{0,2},{1,3},{2,0},{3,1},{4,6},{5,7},{6,4},{7,5},{8,10},{9,11},{10,... | collective-permute-start | bytes 626696 | tf_op jit(solution)/shard_map/ppermute | solution.py:268
  135.5 17.7 %collective-permute-start.7 = (bf16[48,2176]{1,0:T(8,128)(2,1)S(1)}, bf16[48,2176]{1,0:T(8,128)(2,1)S(1)}, u32[]{:S(2)}, u32[]{:S(2)}) collective-permute-start(bf16[48,2176]{1,0:T(8,128)(2,1)S(1)} %get-tuple-element.33), channel_id=1, source_target_pairs={{0,4},{1,5},{2,6},{3,7},{4,0},{5,1},{6,2},{7,3},{8,12},{9,13},{10,... | collective-permute-start | bytes 626696 | tf_op jit(solution)/shard_map/ppermute | solution.py:268
  140.3 12.8 %collective-permute-start.8 = (bf16[48,2176]{1,0:T(8,128)(2,1)S(1)}, bf16[48,2176]{1,0:T(8,128)(2,1)S(1)}, u32[]{:S(2)}, u32[]{:S(2)}) collective-permute-start(bf16[48,2176]{1,0:T(8,128)(2,1)S(1)} %get-tuple-element.34), channel_id=1, source_target_pairs={{0,6},{1,7},{2,4},{3,5},{4,2},{5,3},{6,0},{7,1},{8,14},{9,15},{10,... | collective-permute-start | bytes 626696 | tf_op jit(solution)/shard_map/ppermute | solution.py:268
  144.7 8.4 %collective-permute-start.9 = (bf16[48,2176]{1,0:T(8,128)(2,1)S(1)}, bf16[48,2176]{1,0:T(8,128)(2,1)S(1)}, u32[]{:S(2)}, u32[]{:S(2)}) collective-permute-start(bf16[48,2176]{1,0:T(8,128)(2,1)S(1)} %get-tuple-element.35), channel_id=1, source_target_pairs={{0,8},{1,9},{2,10},{3,11},{4,12},{5,13},{6,14},{7,15},{8,0},{9,1},... | collective-permute-start | bytes 626696 | tf_op jit(solution)/shard_map/ppermute | solution.py:268
  153.2 3.2 %collective-permute-start.13 = (bf16[192,2176]{1,0:T(8,128)(2,1)S(1)}, bf16[192,2176]{1,0:T(8,128)(2,1)}, u32[]{:S(2)}, u32[]{:S(2)}) collective-permute-start(bf16[192,2176]{1,0:T(8,128)(2,1)S(1)} %shard_map.103), channel_id=1, source_target_pairs={{0,1},{1,0},{2,3},{3,2},{4,5},{5,4},{6,7},{7,6},{8,9},{9,8},{10,11... | collective-permute-start | bytes 2506760 | tf_op jit(solution)/shard_map/ppermute | solution.py:268
  155.9 11.2 %collective-permute-start.4 = (bf16[16,3,64,256]{3,2,1,0:T(8,128)(2,1)}, bf16[16,3,64,256]{3,2,1,0:T(8,128)(2,1)}, u32[]{:S(2)}, u32[]{:S(2)}) collective-permute-start(bf16[16,3,64,256]{3,2,1,0:T(8,128)(2,1)} %pad_maximum_fusion.1), channel_id=1, source_target_pairs={{0,1},{1,0},{2,3},{3,2},{4,5},{5,4},{6,7},{7,6},{8,9},{9,8},{10,11... | collective-permute-start | bytes 4718600 | tf_op jit(solution)/shard_map/ppermute | solution.py:268
  166.9 8.9 %collective-permute-start.14 = (bf16[192,2048]{1,0:T(8,128)(2,1)}, bf16[192,2048]{1,0:T(8,128)(2,1)S(1)}, u32[]{:S(2)}, u32[]{:S(2)}) collective-permute-start(bf16[192,2048]{1,0:T(8,128)(2,1)} %get-tuple-element.40), channel_id=1, source_target_pairs={{0,1},{1,0},{2,3},{3,2},{4,5},{5,4},{6,7},{7,6},{8,9},{9,8},{10,11... | collective-permute-start | bytes 2359304 | tf_op jit(solution)/shard_map/ppermute | solution.py:268
  174.8 36.9 %copy-start.3 = (f32[128,2048]{1,0:T(8,128)S(1)}, f32[128,2048]{1,0:T(8,128)}, u32[]{:S(2)}) copy-start(f32[128,2048]{1,0:T(8,128)} %copy-done.2) | copy-start | bytes 3145732
  174.8 36.9 %copy-start.17 = (bf16[256,384]{1,0:T(8,128)(2,1)S(1)}, bf16[256,384]{1,0:T(8,128)(2,1)}, u32[]{:S(2)}) copy-start(bf16[256,384]{1,0:T(8,128)(2,1)} %copy-done.16) | copy-start | bytes 589828
  175.5 36.9 %collective-permute-start.24 = (bf16[128,2048]{1,0:T(8,128)(2,1)S(1)}, bf16[128,2048]{1,0:T(8,128)(2,1)S(1)}, u32[]{:S(2)}, u32[]{:S(2)}) collective-permute-start(bf16[128,2048]{1,0:T(8,128)(2,1)S(1)} %shard_map.110), channel_id=1, source_target_pairs={{0,16},{1,17},{2,18},{3,19},{4,20},{5,21},{6,22},{7,23},{8,24},{9,... | collective-permute-start | bytes 1572872 | tf_op jit(solution)/shard_map/ppermute | solution.py:268
  176.0 8.0 %collective-permute-start.15 = (bf16[48,2048]{1,0:T(8,128)(2,1)S(1)}, bf16[48,2048]{1,0:T(8,128)(2,1)S(1)}, u32[]{:S(2)}, u32[]{:S(2)}) collective-permute-start(bf16[48,2048]{1,0:T(8,128)(2,1)S(1)} %get-tuple-element.42), channel_id=1, source_target_pairs={{0,2},{1,3},{2,0},{3,1},{4,6},{5,7},{6,4},{7,5},{8,10},{9,11},{10,... | collective-permute-start | bytes 589832 | tf_op jit(solution)/shard_map/ppermute | solution.py:268
  178.3 10.4 %collective-permute-start.16 = (bf16[48,2048]{1,0:T(8,128)(2,1)S(1)}, bf16[48,2048]{1,0:T(8,128)(2,1)S(1)}, u32[]{:S(2)}, u32[]{:S(2)}) collective-permute-start(bf16[48,2048]{1,0:T(8,128)(2,1)S(1)} %get-tuple-element.43), channel_id=1, source_target_pairs={{0,4},{1,5},{2,6},{3,7},{4,0},{5,1},{6,2},{7,3},{8,12},{9,13},{10,... | collective-permute-start | bytes 589832 | tf_op jit(solution)/shard_map/ppermute | solution.py:268
  180.0 14.5 %collective-permute-start.17 = (bf16[48,2048]{1,0:T(8,128)(2,1)S(1)}, bf16[48,2048]{1,0:T(8,128)(2,1)S(1)}, u32[]{:S(2)}, u32[]{:S(2)}) collective-permute-start(bf16[48,2048]{1,0:T(8,128)(2,1)S(1)} %get-tuple-element.44), channel_id=1, source_target_pairs={{0,6},{1,7},{2,4},{3,5},{4,2},{5,3},{6,0},{7,1},{8,14},{9,15},{10,... | collective-permute-start | bytes 589832 | tf_op jit(solution)/shard_map/ppermute | solution.py:268
  181.4 13.1 %collective-permute-start.18 = (bf16[48,2048]{1,0:T(8,128)(2,1)S(1)}, bf16[48,2048]{1,0:T(8,128)(2,1)S(1)}, u32[]{:S(2)}, u32[]{:S(2)}) collective-permute-start(bf16[48,2048]{1,0:T(8,128)(2,1)S(1)} %get-tuple-element.45), channel_id=1, source_target_pairs={{0,8},{1,9},{2,10},{3,11},{4,12},{5,13},{6,14},{7,15},{8,0},{9,1},... | collective-permute-start | bytes 589832 | tf_op jit(solution)/shard_map/ppermute | solution.py:268
  184.0 20.1 %collective-permute-start.19 = (bf16[48,2048]{1,0:T(8,128)(2,1)S(1)}, bf16[48,2048]{1,0:T(8,128)(2,1)S(1)}, u32[]{:S(2)}, u32[]{:S(2)}) collective-permute-start(bf16[48,2048]{1,0:T(8,128)(2,1)S(1)} %get-tuple-element.46), channel_id=1, source_target_pairs={{0,10},{1,11},{2,8},{3,9},{4,14},{5,15},{6,12},{7,13},{8,2},{9,3},... | collective-permute-start | bytes 589832 | tf_op jit(solution)/shard_map/ppermute | solution.py:268
  188.7 19.5 %collective-permute-start.20 = (bf16[48,2048]{1,0:T(8,128)(2,1)S(1)}, bf16[48,2048]{1,0:T(8,128)(2,1)S(1)}, u32[]{:S(2)}, u32[]{:S(2)}) collective-permute-start(bf16[48,2048]{1,0:T(8,128)(2,1)S(1)} %get-tuple-element.47), channel_id=1, source_target_pairs={{0,12},{1,13},{2,14},{3,15},{4,8},{5,9},{6,10},{7,11},{8,4},{9,5},... | collective-permute-start | bytes 589832 | tf_op jit(solution)/shard_map/ppermute | solution.py:268
  194.5 17.1 %collective-permute-start.21 = (bf16[48,2048]{1,0:T(8,128)(2,1)S(1)}, bf16[48,2048]{1,0:T(8,128)(2,1)S(1)}, u32[]{:S(2)}, u32[]{:S(2)}) collective-permute-start(bf16[48,2048]{1,0:T(8,128)(2,1)S(1)} %get-tuple-element.48), channel_id=1, source_target_pairs={{0,14},{1,15},{2,12},{3,13},{4,10},{5,11},{6,8},{7,9},{8,6},{9,7},... | collective-permute-start | bytes 589832 | tf_op jit(solution)/shard_map/ppermute | solution.py:268
  (23 other events, 135.5 us)

commit v3 on v2

--- a/solution.py
+++ b/solution.py
@@ -203,15 +203,15 @@
     )(w_gate, w_up, w_down.reshape(experts * hidden, width), *rows)
 
 
-def shared_kernel(me_ref, parts_ref, own_ref, other_ref, out_own_ref, out_other_ref,
+def shared_kernel(me_ref, near_ref, far_ref, own_ref, other_ref, out_own_ref, out_other_ref,
                   gate_ref, up_ref, down_ref, *, offsets):
-    me = me_ref[0]
-    block = parts_ref.shape[2]
-    for place, offset in enumerate(offsets):
-        start = pl.multiple_of((me ^ offset) * block, block)
-        gate_ref[pl.ds(start, block), :] = parts_ref[place, 0]
-        up_ref[pl.ds(start, block), :] = parts_ref[place, 1]
-        down_ref[pl.ds(start, block), :] = parts_ref[place, 2]
+    block = near_ref.shape[2]
+    for parts_ref, me in ((near_ref, me_ref[0]), (far_ref, me_ref[0] ^ 1)):
+        for place, offset in enumerate(offsets):
+            start = pl.multiple_of((me ^ offset) * block, block)
+            gate_ref[pl.ds(start, block), :] = parts_ref[place, 0]
+            up_ref[pl.ds(start, block), :] = parts_ref[place, 1]
+            down_ref[pl.ds(start, block), :] = parts_ref[place, 2]
     for x_ref, out_ref in ((own_ref, out_own_ref), (other_ref, out_other_ref)):
         x = x_ref[...]
         gate_val = jnp.dot(x, gate_ref[...], preferred_element_type=F32)
@@ -286,7 +286,7 @@
     parts = jnp.stack([shared_gate, shared_up, shared_down.T])[None]
     cut = parts.shape[3] // 2
     offsets = [0]
-    for bit in shared_steps(devices):
+    for bit in shared_steps(devices)[:-1]:
         if bit == half:
             low, high = parts[..., :cut], parts[..., cut:]
             mine = jnp.where(side == 0, low, high)
@@ -295,6 +295,7 @@
             mine = theirs = parts
         parts = jnp.concatenate([mine, exchange(theirs, bit)], axis=0)
         offsets += [offset ^ bit for offset in offsets]
+    far_parts = exchange(parts, 1)
 
     ids, weights = expert_ids.T, gate_weights.T
     ids_other = exchange(ids, half)
@@ -339,7 +340,7 @@
     shared_own, shared_other = call(
         functools.partial(shared_kernel, offsets=tuple(offsets)),
         (shape, shape),
-        (me.reshape(1), parts, normed, normed_other),
+        (me.reshape(1), parts, far_parts, normed, normed_other),
         flops=12 * count * width * cut,
         scratch_shapes=[full, full, full],
     )
@@ -357,10 +358,8 @@
 
 def shared_steps(devices):
     half = devices // 2
-    bits = [1 << b for b in range(devices.bit_length() - 3, -1, -1)]
-    early = [bit for bit in bits if 2 <= bit <= 4]
-    late = [bit for bit in bits if 4 < bit]
-    return early + [half] + late + [1]
+    bits = [1 << b for b in range(devices.bit_length() - 3, 0, -1)]
+    return [half] + bits[1:] + [bits[0], 1]
 
 
 def solution(mesh):

time: 214 us -> 203 us (0.949)
  starting transfers between devices: 49.7 us -> 39.2 us
  other arithmetic: 6.45 us -> 1.76 us
  local copies, waits for them, and re-layouts: 7.3 us -> 10.6 us
    ppermute x25, starting transfers between devices: 41.1 us -> 26.8 us  [exchange(): return lax.ppermute(array, 'ep', [(i, i ^ bit) for i in range(devices)])]
    concatenate x5 -> x3, other arithmetic: 5.48 us -> 0.91 us  [per_device(): parts = jnp.concatenate([mine, exchange(theirs, bit)], axis=0)]
    all_to_all x2, starting transfers between devices: 8.58 us -> 12.4 us  [within(): lax.all_to_all(array, 'ep', 0, 0, axis_index_groups=groups, tiled=True)]
    unnamed x56 -> x55, local copies, waits for them, and re-layouts: 7.3 us -> 9.67 us
  transfers between devices with their start and end apart: 27 -> 27, of which waited for: 14 -> 16; matrix products, arithmetic and copies ran while one was open for 3% -> 2% of each run, Pallas kernels for 12% -> 14%
where the time goes in v3:
time: 203 us; the launch traced here: 202 us
  waiting for transfers between devices  119 us (59%)
  starting transfers between devices  39.2 us (19%)
  Pallas kernels  31 us (15%)
  local copies, waits for them, and re-layouts  10.6 us (5%)
    ppermute x25, waiting for transfers between devices, exchange(): return lax.ppermute(array, 'ep', [(i, i ^ bit) for i in range(devices)])  119 us
    ppermute x25, starting transfers between devices, exchange(): return lax.ppermute(array, 'ep', [(i, i ^ bit) for i in range(devices)])  26.8 us
    pallas_call x2, Pallas kernels, run_experts(): pl.pallas_call(functools.partial(expert_kernel, takes=tuple(takes), resul...  20.7 us
    all_to_all x2, starting transfers between devices, within(): lax.all_to_all(array, 'ep', 0, 0, axis_index_groups=groups, tiled=True)  12.4 us
    pallas_call x10, Pallas kernels, call(): pl.pallas_call(kernel, in_specs=[SMEM] * scalars + [VMEM] * (len(args) -...  10.3 us
    unnamed x55, local copies, waits for them, and re-layouts  9.67 us
  transfers between devices with their start and end apart: 27, of which 16 were waited for; matrix products, arithmetic and copies ran while one was open for 2% of the time, Pallas kernels for 14%

profile of v3, /device:TPU:0, one launch (start us, length us, event | category | flops | bytes accessed | tf_op | source)
XLA Modules:
  0.0 202.4 jit_solution(5435325945240821852)
XLA Ops:
  2.0 4.1 %collective-permute-start.5 = (bf16[128,2048]{1,0:T(8,128)(2,1)S(1)}, bf16[128,2048]{1,0:T(8,128)(2,1)S(1)}, u32[]{:S(2)}, u32[]{:S(2)}) collective-permute-start(bf16[128,2048]{1,0:T(8,128)(2,1)S(1)} %shard_map.100.x_ref.own_ref), channel_id=1, source_target_pairs={{0,16},{1,17},{2,18},{3,19},{4,20},{5,21},{6,22},{7,23},{8,24},{9,... | collective-permute-start | bytes 1572872 | tf_op jit(solution)/shard_map/ppermute | solution.py:268
  6.2 2.8 %collective-permute-start.23 = (f32[4,128]{1,0:T(4,128)}, f32[4,128]{1,0:T(4,128)S(1)}, u32[]{:S(2)}, u32[]{:S(2)}) collective-permute-start(f32[4,128]{1,0:T(4,128)} %bitcast.22), channel_id=1, source_target_pairs={{0,16},{1,17},{2,18},{3,19},{4,20},{5,21},{6,22},{7,23},{8,24},{9,... | collective-permute-start | bytes 6152 | tf_op jit(solution)/shard_map/ppermute | solution.py:268
  9.1 20.3 %collective-permute-done.22.ids_ref = s32[4,128]{1,0:T(4,128)S(1)} collective-permute-done((s32[4,128]{1,0:T(4,128)}, s32[4,128]{1,0:T(4,128)S(1)}, u32[]{:S(2)}, u32[]{:S(2)}) %collective-permute-start.22) | collective-permute-done | bytes 2080 | tf_op jit(solution)/shard_map/ppermute | solution.py:268
  31.1 1.8 shard_map.108
  32.9 4.5 %all-to-all-start = ((bf16[16,24,2176]{2,1,0:T(8,128)(2,1)}), bf16[16,24,2176]{2,1,0:T(8,128)(2,1)}, u32[]{:S(2)}, u32[]{:S(2)}) async-start(bf16[16,24,2176]{2,1,0:T(8,128)(2,1)} %bitcast.12), calls=%async_computation | async-start | bytes 3342336 | tf_op jit(solution)/shard_map/all_to_all | solution.py:271
  38.2 3.0 %collective-permute-start = (bf16[1,3,64,256]{3,2,1,0:T(8,128)(2,1)S(1)}, bf16[1,3,64,256]{3,2,1,0:T(8,128)(2,1)S(1)}, u32[]{:S(2)}, u32[]{:S(2)}) collective-permute-start(bf16[1,3,64,256]{3,2,1,0:T(8,128)(2,1)S(1)} %get-tuple-element.55), channel_id=1, source_target_pairs={{0,16},{1,17},{2,18},{3,19},{4,20},{5,21},{6,22},{7,23},{8,24},{9,... | collective-permute-start | bytes 294920 | tf_op jit(solution)/shard_map/ppermute | solution.py:268
  41.2 17.7 %collective-permute-done = bf16[1,3,64,256]{3,2,1,0:T(8,128)(2,1)S(1)} collective-permute-done((bf16[1,3,64,256]{3,2,1,0:T(8,128)(2,1)S(1)}, bf16[1,3,64,256]{3,2,1,0:T(8,128)(2,1)S(1)}, u32[]{:S(2)}, u32[]{:S(2)}) %collective-permute-start) | collective-permute-done | bytes 98336 | tf_op jit(solution)/shard_map/ppermute | solution.py:268
  58.9 2.5 %collective-permute-start.1 = (bf16[2,3,64,256]{3,2,1,0:T(8,128)(2,1)S(1)}, bf16[2,3,64,256]{3,2,1,0:T(8,128)(2,1)S(1)}, u32[]{:S(2)}, u32[]{:S(2)}) collective-permute-start(bf16[2,3,64,256]{3,2,1,0:T(8,128)(2,1)S(1)} %pad_maximum_fusion.2), channel_id=1, source_target_pairs={{0,4},{1,5},{2,6},{3,7},{4,0},{5,1},{6,2},{7,3},{8,12},{9,13},{10,... | collective-permute-start | bytes 589832 | tf_op jit(solution)/shard_map/ppermute | solution.py:268
  61.3 5.9 %collective-permute-done.1 = bf16[2,3,64,256]{3,2,1,0:T(8,128)(2,1)S(1)} collective-permute-done((bf16[2,3,64,256]{3,2,1,0:T(8,128)(2,1)S(1)}, bf16[2,3,64,256]{3,2,1,0:T(8,128)(2,1)S(1)}, u32[]{:S(2)}, u32[]{:S(2)}) %collective-permute-start.1) | collective-permute-done | bytes 196640 | tf_op jit(solution)/shard_map/ppermute | solution.py:268
  68.1 10.2 %shard_map.109 = bf16[384,2048]{1,0:T(8,128)(2,1)} custom-call(bf16[2,2048,512]{2,1,0:T(8,128)(2,1)} %gate_ref.3, bf16[2,2048,512]{2,1,0:T(8,128)(2,1)} %up_ref.3, bf16[1024,2048]{1,0:T(8,128)(2,1)} %bitcast.28, bf16[384,2176]{1,0:T(8,128)(2,1)} %bitcast.13.refs_0_), custom_call_target="tpu_custom_call" | custom-call | flops 4831838208 | bytes 15728640 | tf_op jit(solution)/shard_map/pallas_call | solution.py:189
  78.3 7.9 %all-to-all-start.1 = ((bf16[16,24,2048]{2,1,0:T(8,128)(2,1)}), bf16[16,24,2048]{2,1,0:T(8,128)(2,1)S(1)}, u32[]{:S(2)}, u32[]{:S(2)}) async-start(bf16[16,24,2048]{2,1,0:T(8,128)(2,1)} %bitcast.24), calls=%async_computation.1 | async-start | bytes 3145728 | tf_op jit(solution)/shard_map/all_to_all | solution.py:271
  86.4 2.0 collective-permute-start.3
  88.4 1.3 shard_map.101
  90.4 1.5 collective-permute-start.6
  91.9 1.5 collective-permute-start.7
  94.3 19.2 %collective-permute-done.6.refs_1_ = bf16[48,2176]{1,0:T(8,128)(2,1)S(1)} collective-permute-done((bf16[48,2176]{1,0:T(8,128)(2,1)S(1)}, bf16[48,2176]{1,0:T(8,128)(2,1)S(1)}, u32[]{:S(2)}, u32[]{:S(2)}) %collective-permute-start.6) | collective-permute-done | bytes 208928 | tf_op jit(solution)/shard_map/ppermute | solution.py:268
  115.0 2.1 %collective-permute-done.8.refs_3_ = bf16[48,2176]{1,0:T(8,128)(2,1)S(1)} collective-permute-done((bf16[48,2176]{1,0:T(8,128)(2,1)S(1)}, bf16[48,2176]{1,0:T(8,128)(2,1)S(1)}, u32[]{:S(2)}, u32[]{:S(2)}) %collective-permute-start.8) | collective-permute-done | bytes 208928 | tf_op jit(solution)/shard_map/ppermute | solution.py:268
  117.2 1.5 collective-permute-start.12
  119.3 8.9 %collective-permute-done.9.refs_4_ = bf16[48,2176]{1,0:T(8,128)(2,1)S(1)} collective-permute-done((bf16[48,2176]{1,0:T(8,128)(2,1)S(1)}, bf16[48,2176]{1,0:T(8,128)(2,1)S(1)}, u32[]{:S(2)}, u32[]{:S(2)}) %collective-permute-start.9) | collective-permute-done | bytes 208928 | tf_op jit(solution)/shard_map/ppermute | solution.py:268
  128.2 6.4 %collective-permute-done.10.refs_5_ = bf16[48,2176]{1,0:T(8,128)(2,1)S(1)} collective-permute-done((bf16[48,2176]{1,0:T(8,128)(2,1)S(1)}, bf16[48,2176]{1,0:T(8,128)(2,1)S(1)}, u32[]{:S(2)}, u32[]{:S(2)}) %collective-permute-start.10) | collective-permute-done | bytes 208928 | tf_op jit(solution)/shard_map/ppermute | solution.py:268
  134.6 4.6 %collective-permute-done.11.refs_6_ = bf16[48,2176]{1,0:T(8,128)(2,1)S(1)} collective-permute-done((bf16[48,2176]{1,0:T(8,128)(2,1)S(1)}, bf16[48,2176]{1,0:T(8,128)(2,1)S(1)}, u32[]{:S(2)}, u32[]{:S(2)}) %collective-permute-start.11) | collective-permute-done | bytes 208928 | tf_op jit(solution)/shard_map/ppermute | solution.py:268
  139.2 4.3 %collective-permute-done.12.refs_7_ = bf16[48,2176]{1,0:T(8,128)(2,1)S(1)} collective-permute-done((bf16[48,2176]{1,0:T(8,128)(2,1)S(1)}, bf16[48,2176]{1,0:T(8,128)(2,1)S(1)}, u32[]{:S(2)}, u32[]{:S(2)}) %collective-permute-start.12) | collective-permute-done | bytes 208928 | tf_op jit(solution)/shard_map/ppermute | solution.py:268
  146.6 10.5 %shard_map.104 = (bf16[192,2048]{1,0:T(8,128)(2,1)}, bf16[192,2048]{1,0:T(8,128)(2,1)}) custom-call(bf16[2,2048,512]{2,1,0:T(8,128)(2,1)} %gate_ref.3, bf16[2,2048,512]{2,1,0:T(8,128)(2,1)} %up_ref.3, bf16[1024,2048]{1,0:T(8,128)(2,1)} %bitcast.29, bf16[48,2176]{1,0:T(8,128)(2,1)} %copy-done.6, bf16[48,2176]{1,0:T(8,128)(2,1)} %copy-done.7, ...), custom_call_target="tpu_custom_call" | custom-call | flops 4831838208 | bytes 15728640 | tf_op jit(solution)/shard_map/pallas_call | solution.py:189
  157.3 3.6 %shard_map.102 = (f32[128,2048]{1,0:T(8,128)S(1)}, f32[128,2048]{1,0:T(8,128)S(1)}) custom-call(s32[1]{0:T(128)} %bitcast.5.me_ref, bf16[16,3,64,256]{3,2,1,0:T(8,128)(2,1)} %constant_dynamic-update-slice_fusion.near_ref, bf16[16,3,64,256]{3,2,1,0:T(8,128)(2,1)} %collective-permute-done.4.far_ref, bf16[128,2048]{1,0:T(8,128)(2,1)S(1)} %shard_map.100.x_ref.own_ref, ...), custom_call_target="tpu_custom_call" | custom-call | flops 805306368 | bytes 6291460 | tf_op jit(solution)/shard_map/pallas_call | solution.py:228
  162.8 1.2 copy-done.1
  167.7 2.0 collective-permute-start.17
  170.2 3.8 %collective-permute-done.15.refs_1_ = bf16[48,2048]{1,0:T(8,128)(2,1)S(1)} collective-permute-done((bf16[48,2048]{1,0:T(8,128)(2,1)S(1)}, bf16[48,2048]{1,0:T(8,128)(2,1)S(1)}, u32[]{:S(2)}, u32[]{:S(2)}) %collective-permute-start.15) | collective-permute-done | bytes 196640 | tf_op jit(solution)/shard_map/ppermute | solution.py:268
  174.5 3.0 %collective-permute-done.16.refs_2_ = bf16[48,2048]{1,0:T(8,128)(2,1)S(1)} collective-permute-done((bf16[48,2048]{1,0:T(8,128)(2,1)S(1)}, bf16[48,2048]{1,0:T(8,128)(2,1)S(1)}, u32[]{:S(2)}, u32[]{:S(2)}) %collective-permute-start.16) | collective-permute-done | bytes 196640 | tf_op jit(solution)/shard_map/ppermute | solution.py:268
  177.5 3.8 %collective-permute-done.17.refs_3_ = bf16[48,2048]{1,0:T(8,128)(2,1)S(1)} collective-permute-done((bf16[48,2048]{1,0:T(8,128)(2,1)S(1)}, bf16[48,2048]{1,0:T(8,128)(2,1)S(1)}, u32[]{:S(2)}, u32[]{:S(2)}) %collective-permute-start.17) | collective-permute-done | bytes 196640 | tf_op jit(solution)/shard_map/ppermute | solution.py:268
  182.3 11.1 %collective-permute-done.19.refs_5_ = bf16[48,2048]{1,0:T(8,128)(2,1)S(1)} collective-permute-done((bf16[48,2048]{1,0:T(8,128)(2,1)S(1)}, bf16[48,2048]{1,0:T(8,128)(2,1)S(1)}, u32[]{:S(2)}, u32[]{:S(2)}) %collective-permute-start.19) | collective-permute-done | bytes 196640 | tf_op jit(solution)/shard_map/ppermute | solution.py:268
  193.4 4.1 %collective-permute-done.20.refs_6_ = bf16[48,2048]{1,0:T(8,128)(2,1)S(1)} collective-permute-done((bf16[48,2048]{1,0:T(8,128)(2,1)S(1)}, bf16[48,2048]{1,0:T(8,128)(2,1)S(1)}, u32[]{:S(2)}, u32[]{:S(2)}) %collective-permute-start.20) | collective-permute-done | bytes 196640 | tf_op jit(solution)/shard_map/ppermute | solution.py:268
  197.5 3.3 %collective-permute-done.21.refs_7_ = bf16[48,2048]{1,0:T(8,128)(2,1)S(1)} collective-permute-done((bf16[48,2048]{1,0:T(8,128)(2,1)S(1)}, bf16[48,2048]{1,0:T(8,128)(2,1)S(1)}, u32[]{:S(2)}, u32[]{:S(2)}) %collective-permute-start.21) | collective-permute-done | bytes 196640 | tf_op jit(solution)/shard_map/ppermute | solution.py:268
  (97 shorter events, 21.8 us)
Async XLA Ops:
  2.0 29.2 %collective-permute-start.5 = (bf16[128,2048]{1,0:T(8,128)(2,1)S(1)}, bf16[128,2048]{1,0:T(8,128)(2,1)S(1)}, u32[]{:S(2)}, u32[]{:S(2)}) collective-permute-start(bf16[128,2048]{1,0:T(8,128)(2,1)S(1)} %shard_map.100.x_ref.own_ref), channel_id=1, source_target_pairs={{0,16},{1,17},{2,18},{3,19},{4,20},{5,21},{6,22},{7,23},{8,24},{9,... | collective-permute-start | bytes 1572872 | tf_op jit(solution)/shard_map/ppermute | solution.py:268
  6.1 23.3 %collective-permute-start.22 = (s32[4,128]{1,0:T(4,128)}, s32[4,128]{1,0:T(4,128)S(1)}, u32[]{:S(2)}, u32[]{:S(2)}) collective-permute-start(s32[4,128]{1,0:T(4,128)} %bitcast.20), channel_id=1, source_target_pairs={{0,16},{1,17},{2,18},{3,19},{4,20},{5,21},{6,22},{7,23},{8,24},{9,... | collective-permute-start | bytes 6152 | tf_op jit(solution)/shard_map/ppermute | solution.py:268
  6.2 23.3 %collective-permute-start.23 = (f32[4,128]{1,0:T(4,128)}, f32[4,128]{1,0:T(4,128)S(1)}, u32[]{:S(2)}, u32[]{:S(2)}) collective-permute-start(f32[4,128]{1,0:T(4,128)} %bitcast.22), channel_id=1, source_target_pairs={{0,16},{1,17},{2,18},{3,19},{4,20},{5,21},{6,22},{7,23},{8,24},{9,... | collective-permute-start | bytes 6152 | tf_op jit(solution)/shard_map/ppermute | solution.py:268
  32.9 35.2 %all-to-all-start = ((bf16[16,24,2176]{2,1,0:T(8,128)(2,1)}), bf16[16,24,2176]{2,1,0:T(8,128)(2,1)}, u32[]{:S(2)}, u32[]{:S(2)}) async-start(bf16[16,24,2176]{2,1,0:T(8,128)(2,1)} %bitcast.12), calls=%async_computation | async-start | bytes 3342336 | tf_op jit(solution)/shard_map/all_to_all | solution.py:271
  38.2 20.7 %collective-permute-start = (bf16[1,3,64,256]{3,2,1,0:T(8,128)(2,1)S(1)}, bf16[1,3,64,256]{3,2,1,0:T(8,128)(2,1)S(1)}, u32[]{:S(2)}, u32[]{:S(2)}) collective-permute-start(bf16[1,3,64,256]{3,2,1,0:T(8,128)(2,1)S(1)} %get-tuple-element.55), channel_id=1, source_target_pairs={{0,16},{1,17},{2,18},{3,19},{4,20},{5,21},{6,22},{7,23},{8,24},{9,... | collective-permute-start | bytes 294920 | tf_op jit(solution)/shard_map/ppermute | solution.py:268
  58.9 8.3 %collective-permute-start.1 = (bf16[2,3,64,256]{3,2,1,0:T(8,128)(2,1)S(1)}, bf16[2,3,64,256]{3,2,1,0:T(8,128)(2,1)S(1)}, u32[]{:S(2)}, u32[]{:S(2)}) collective-permute-start(bf16[2,3,64,256]{3,2,1,0:T(8,128)(2,1)S(1)} %pad_maximum_fusion.2), channel_id=1, source_target_pairs={{0,4},{1,5},{2,6},{3,7},{4,0},{5,1},{6,2},{7,3},{8,12},{9,13},{10,... | collective-permute-start | bytes 589832 | tf_op jit(solution)/shard_map/ppermute | solution.py:268
  68.0 18.2 %collective-permute-start.2 = (bf16[4,3,64,256]{3,2,1,0:T(8,128)(2,1)}, bf16[4,3,64,256]{3,2,1,0:T(8,128)(2,1)S(1)}, u32[]{:S(2)}, u32[]{:S(2)}) collective-permute-start(bf16[4,3,64,256]{3,2,1,0:T(8,128)(2,1)} %pad_maximum_fusion.1), channel_id=1, source_target_pairs={{0,2},{1,3},{2,0},{3,1},{4,6},{5,7},{6,4},{7,5},{8,10},{9,11},{10,... | collective-permute-start | bytes 1179656 | tf_op jit(solution)/shard_map/ppermute | solution.py:268
  78.3 84.5 %all-to-all-start.1 = ((bf16[16,24,2048]{2,1,0:T(8,128)(2,1)}), bf16[16,24,2048]{2,1,0:T(8,128)(2,1)S(1)}, u32[]{:S(2)}, u32[]{:S(2)}) async-start(bf16[16,24,2048]{2,1,0:T(8,128)(2,1)} %bitcast.24), calls=%async_computation.1 | async-start | bytes 3145728 | tf_op jit(solution)/shard_map/all_to_all | solution.py:271
  86.4 58.8 %collective-permute-start.3 = (bf16[8,3,64,256]{3,2,1,0:T(8,128)(2,1)S(1)}, bf16[8,3,64,256]{3,2,1,0:T(8,128)(2,1)S(1)}, u32[]{:S(2)}, u32[]{:S(2)}) collective-permute-start(bf16[8,3,64,256]{3,2,1,0:T(8,128)(2,1)S(1)} %pad_maximum_fusion), channel_id=1, source_target_pairs={{0,8},{1,9},{2,10},{3,11},{4,12},{5,13},{6,14},{7,15},{8,0},{9,1},... | collective-permute-start | bytes 2359304 | tf_op jit(solution)/shard_map/ppermute | solution.py:268
  88.4 55.2 %copy-start.22 = (bf16[2,3,64,256]{3,2,1,0:T(8,128)(2,1)S(1)}, bf16[2,3,64,256]{3,2,1,0:T(8,128)(2,1)}, u32[]{:S(2)}) copy-start(bf16[2,3,64,256]{3,2,1,0:T(8,128)(2,1)} %copy-done.21) | copy-start | bytes 589828
  90.4 54.7 %copy-start.6 = (bf16[48,2176]{1,0:T(8,128)(2,1)}, bf16[48,2176]{1,0:T(8,128)(2,1)S(1)}, u32[]{:S(2)}) copy-start(bf16[48,2176]{1,0:T(8,128)(2,1)S(1)} %get-tuple-element.31.refs_0_) | copy-start | bytes 626692
  90.4 23.1 %collective-permute-start.6 = (bf16[48,2176]{1,0:T(8,128)(2,1)S(1)}, bf16[48,2176]{1,0:T(8,128)(2,1)S(1)}, u32[]{:S(2)}, u32[]{:S(2)}) collective-permute-start(bf16[48,2176]{1,0:T(8,128)(2,1)S(1)} %get-tuple-element.32), channel_id=1, source_target_pairs={{0,2},{1,3},{2,0},{3,1},{4,6},{5,7},{6,4},{7,5},{8,10},{9,11},{10,... | collective-permute-start | bytes 626696 | tf_op jit(solution)/shard_map/ppermute | solution.py:268
  91.9 22.0 %collective-permute-start.7 = (bf16[48,2176]{1,0:T(8,128)(2,1)S(1)}, bf16[48,2176]{1,0:T(8,128)(2,1)S(1)}, u32[]{:S(2)}, u32[]{:S(2)}) collective-permute-start(bf16[48,2176]{1,0:T(8,128)(2,1)S(1)} %get-tuple-element.33), channel_id=1, source_target_pairs={{0,4},{1,5},{2,6},{3,7},{4,0},{5,1},{6,2},{7,3},{8,12},{9,13},{10,... | collective-permute-start | bytes 626696 | tf_op jit(solution)/shard_map/ppermute | solution.py:268
  93.4 23.8 %collective-permute-start.8 = (bf16[48,2176]{1,0:T(8,128)(2,1)S(1)}, bf16[48,2176]{1,0:T(8,128)(2,1)S(1)}, u32[]{:S(2)}, u32[]{:S(2)}) collective-permute-start(bf16[48,2176]{1,0:T(8,128)(2,1)S(1)} %get-tuple-element.34), channel_id=1, source_target_pairs={{0,6},{1,7},{2,4},{3,5},{4,2},{5,3},{6,0},{7,1},{8,14},{9,15},{10,... | collective-permute-start | bytes 626696 | tf_op jit(solution)/shard_map/ppermute | solution.py:268
  93.9 34.3 %collective-permute-start.9 = (bf16[48,2176]{1,0:T(8,128)(2,1)S(1)}, bf16[48,2176]{1,0:T(8,128)(2,1)S(1)}, u32[]{:S(2)}, u32[]{:S(2)}) collective-permute-start(bf16[48,2176]{1,0:T(8,128)(2,1)S(1)} %get-tuple-element.35), channel_id=1, source_target_pairs={{0,8},{1,9},{2,10},{3,11},{4,12},{5,13},{6,14},{7,15},{8,0},{9,1},... | collective-permute-start | bytes 626696 | tf_op jit(solution)/shard_map/ppermute | solution.py:268
  113.6 31.6 %copy-start.7 = (bf16[48,2176]{1,0:T(8,128)(2,1)}, bf16[48,2176]{1,0:T(8,128)(2,1)S(1)}, u32[]{:S(2)}) copy-start(bf16[48,2176]{1,0:T(8,128)(2,1)S(1)} %collective-permute-done.6.refs_1_) | copy-start | bytes 626692
  113.6 21.0 %collective-permute-start.10 = (bf16[48,2176]{1,0:T(8,128)(2,1)S(1)}, bf16[48,2176]{1,0:T(8,128)(2,1)S(1)}, u32[]{:S(2)}, u32[]{:S(2)}) collective-permute-start(bf16[48,2176]{1,0:T(8,128)(2,1)S(1)} %get-tuple-element.36), channel_id=1, source_target_pairs={{0,10},{1,11},{2,8},{3,9},{4,14},{5,15},{6,12},{7,13},{8,2},{9,3},... | collective-permute-start | bytes 626696 | tf_op jit(solution)/shard_map/ppermute | solution.py:268
  113.9 25.3 %collective-permute-start.11 = (bf16[48,2176]{1,0:T(8,128)(2,1)S(1)}, bf16[48,2176]{1,0:T(8,128)(2,1)S(1)}, u32[]{:S(2)}, u32[]{:S(2)}) collective-permute-start(bf16[48,2176]{1,0:T(8,128)(2,1)S(1)} %get-tuple-element.37), channel_id=1, source_target_pairs={{0,12},{1,13},{2,14},{3,15},{4,8},{5,9},{6,10},{7,11},{8,4},{9,5},... | collective-permute-start | bytes 626696 | tf_op jit(solution)/shard_map/ppermute | solution.py:268
  117.2 26.3 %collective-permute-start.12 = (bf16[48,2176]{1,0:T(8,128)(2,1)S(1)}, bf16[48,2176]{1,0:T(8,128)(2,1)S(1)}, u32[]{:S(2)}, u32[]{:S(2)}) collective-permute-start(bf16[48,2176]{1,0:T(8,128)(2,1)S(1)} %get-tuple-element.38), channel_id=1, source_target_pairs={{0,14},{1,15},{2,12},{3,13},{4,10},{5,11},{6,8},{7,9},{8,6},{9,7},... | collective-permute-start | bytes 626696 | tf_op jit(solution)/shard_map/ppermute | solution.py:268
  143.6 3.1 %collective-permute-start.13 = (bf16[192,2176]{1,0:T(8,128)(2,1)S(1)}, bf16[192,2176]{1,0:T(8,128)(2,1)}, u32[]{:S(2)}, u32[]{:S(2)}) collective-permute-start(bf16[192,2176]{1,0:T(8,128)(2,1)S(1)} %shard_map.103), channel_id=1, source_target_pairs={{0,1},{1,0},{2,3},{3,2},{4,5},{5,4},{6,7},{7,6},{8,9},{9,8},{10,11... | collective-permute-start | bytes 2506760 | tf_op jit(solution)/shard_map/ppermute | solution.py:268
  146.2 11.1 %collective-permute-start.4 = (bf16[16,3,64,256]{3,2,1,0:T(8,128)(2,1)}, bf16[16,3,64,256]{3,2,1,0:T(8,128)(2,1)}, u32[]{:S(2)}, u32[]{:S(2)}) collective-permute-start(bf16[16,3,64,256]{3,2,1,0:T(8,128)(2,1)} %constant_dynamic-update-slice_fusion.near_ref), channel_id=1, source_target_pairs={{0,1},{1,0},{2,3},{3,2},{4,5},{5,4},{6,7},{7,6},{8,9},{9,8},{10,11... | collective-permute-start | bytes 4718600 | tf_op jit(solution)/shard_map/ppermute | solution.py:268
  157.2 8.6 %collective-permute-start.14 = (bf16[192,2048]{1,0:T(8,128)(2,1)}, bf16[192,2048]{1,0:T(8,128)(2,1)S(1)}, u32[]{:S(2)}, u32[]{:S(2)}) collective-permute-start(bf16[192,2048]{1,0:T(8,128)(2,1)} %get-tuple-element.40), channel_id=1, source_target_pairs={{0,1},{1,0},{2,3},{3,2},{4,5},{5,4},{6,7},{7,6},{8,9},{9,8},{10,11... | collective-permute-start | bytes 2359304 | tf_op jit(solution)/shard_map/ppermute | solution.py:268
  165.6 35.2 %copy-start.3 = (f32[128,2048]{1,0:T(8,128)S(1)}, f32[128,2048]{1,0:T(8,128)}, u32[]{:S(2)}) copy-start(f32[128,2048]{1,0:T(8,128)} %copy-done.2) | copy-start | bytes 3145732
  165.7 35.2 %copy-start.17 = (bf16[256,384]{1,0:T(8,128)(2,1)S(1)}, bf16[256,384]{1,0:T(8,128)(2,1)}, u32[]{:S(2)}) copy-start(bf16[256,384]{1,0:T(8,128)(2,1)} %copy-done.16) | copy-start | bytes 589828
  165.7 35.9 %collective-permute-start.24 = (bf16[128,2048]{1,0:T(8,128)(2,1)S(1)}, bf16[128,2048]{1,0:T(8,128)(2,1)S(1)}, u32[]{:S(2)}, u32[]{:S(2)}) collective-permute-start(bf16[128,2048]{1,0:T(8,128)(2,1)S(1)} %shard_map.110), channel_id=1, source_target_pairs={{0,16},{1,17},{2,18},{3,19},{4,20},{5,21},{6,22},{7,23},{8,24},{9,... | collective-permute-start | bytes 1572872 | tf_op jit(solution)/shard_map/ppermute | solution.py:268
  166.2 7.8 %collective-permute-start.15 = (bf16[48,2048]{1,0:T(8,128)(2,1)S(1)}, bf16[48,2048]{1,0:T(8,128)(2,1)S(1)}, u32[]{:S(2)}, u32[]{:S(2)}) collective-permute-start(bf16[48,2048]{1,0:T(8,128)(2,1)S(1)} %get-tuple-element.42), channel_id=1, source_target_pairs={{0,2},{1,3},{2,0},{3,1},{4,6},{5,7},{6,4},{7,5},{8,10},{9,11},{10,... | collective-permute-start | bytes 589832 | tf_op jit(solution)/shard_map/ppermute | solution.py:268
  167.3 10.2 %collective-permute-start.16 = (bf16[48,2048]{1,0:T(8,128)(2,1)S(1)}, bf16[48,2048]{1,0:T(8,128)(2,1)S(1)}, u32[]{:S(2)}, u32[]{:S(2)}) collective-permute-start(bf16[48,2048]{1,0:T(8,128)(2,1)S(1)} %get-tuple-element.43), channel_id=1, source_target_pairs={{0,4},{1,5},{2,6},{3,7},{4,0},{5,1},{6,2},{7,3},{8,12},{9,13},{10,... | collective-permute-start | bytes 589832 | tf_op jit(solution)/shard_map/ppermute | solution.py:268
  167.7 13.6 %collective-permute-start.17 = (bf16[48,2048]{1,0:T(8,128)(2,1)S(1)}, bf16[48,2048]{1,0:T(8,128)(2,1)S(1)}, u32[]{:S(2)}, u32[]{:S(2)}) collective-permute-start(bf16[48,2048]{1,0:T(8,128)(2,1)S(1)} %get-tuple-element.44), channel_id=1, source_target_pairs={{0,6},{1,7},{2,4},{3,5},{4,2},{5,3},{6,0},{7,1},{8,14},{9,15},{10,... | collective-permute-start | bytes 589832 | tf_op jit(solution)/shard_map/ppermute | solution.py:268
  169.7 12.6 %collective-permute-start.18 = (bf16[48,2048]{1,0:T(8,128)(2,1)S(1)}, bf16[48,2048]{1,0:T(8,128)(2,1)S(1)}, u32[]{:S(2)}, u32[]{:S(2)}) collective-permute-start(bf16[48,2048]{1,0:T(8,128)(2,1)S(1)} %get-tuple-element.45), channel_id=1, source_target_pairs={{0,8},{1,9},{2,10},{3,11},{4,12},{5,13},{6,14},{7,15},{8,0},{9,1},... | collective-permute-start | bytes 589832 | tf_op jit(solution)/shard_map/ppermute | solution.py:268
  174.0 19.4 %collective-permute-start.19 = (bf16[48,2048]{1,0:T(8,128)(2,1)S(1)}, bf16[48,2048]{1,0:T(8,128)(2,1)S(1)}, u32[]{:S(2)}, u32[]{:S(2)}) collective-permute-start(bf16[48,2048]{1,0:T(8,128)(2,1)S(1)} %get-tuple-element.46), channel_id=1, source_target_pairs={{0,10},{1,11},{2,8},{3,9},{4,14},{5,15},{6,12},{7,13},{8,2},{9,3},... | collective-permute-start | bytes 589832 | tf_op jit(solution)/shard_map/ppermute | solution.py:268
  177.5 20.0 %collective-permute-start.20 = (bf16[48,2048]{1,0:T(8,128)(2,1)S(1)}, bf16[48,2048]{1,0:T(8,128)(2,1)S(1)}, u32[]{:S(2)}, u32[]{:S(2)}) collective-permute-start(bf16[48,2048]{1,0:T(8,128)(2,1)S(1)} %get-tuple-element.47), channel_id=1, source_target_pairs={{0,12},{1,13},{2,14},{3,15},{4,8},{5,9},{6,10},{7,11},{8,4},{9,5},... | collective-permute-start | bytes 589832 | tf_op jit(solution)/shard_map/ppermute | solution.py:268
  181.3 19.5 %collective-permute-start.21 = (bf16[48,2048]{1,0:T(8,128)(2,1)S(1)}, bf16[48,2048]{1,0:T(8,128)(2,1)S(1)}, u32[]{:S(2)}, u32[]{:S(2)}) collective-permute-start(bf16[48,2048]{1,0:T(8,128)(2,1)S(1)} %get-tuple-element.48), channel_id=1, source_target_pairs={{0,14},{1,15},{2,12},{3,13},{4,10},{5,11},{6,8},{7,9},{8,6},{9,7},... | collective-permute-start | bytes 589832 | tf_op jit(solution)/shard_map/ppermute | solution.py:268
  (21 other events, 139.9 us)

commit v4 on v3

--- a/solution.py
+++ b/solution.py
@@ -203,10 +203,12 @@
     )(w_gate, w_up, w_down.reshape(experts * hidden, width), *rows)
 
 
-def shared_kernel(me_ref, near_ref, far_ref, own_ref, other_ref, out_own_ref, out_other_ref,
-                  gate_ref, up_ref, down_ref, *, offsets):
-    block = near_ref.shape[2]
-    for parts_ref, me in ((near_ref, me_ref[0]), (far_ref, me_ref[0] ^ 1)):
+def shared_kernel(me_ref, *refs, offsets, hops):
+    parts_refs = refs[: len(hops)]
+    own_ref, other_ref, out_own_ref, out_other_ref, gate_ref, up_ref, down_ref = refs[len(hops) :]
+    block = parts_refs[0].shape[2]
+    for parts_ref, hop in zip(parts_refs, hops):
+        me = me_ref[0] ^ hop
         for place, offset in enumerate(offsets):
             start = pl.multiple_of((me ^ offset) * block, block)
             gate_ref[pl.ds(start, block), :] = parts_ref[place, 0]
@@ -286,7 +288,8 @@
     parts = jnp.stack([shared_gate, shared_up, shared_down.T])[None]
     cut = parts.shape[3] // 2
     offsets = [0]
-    for bit in shared_steps(devices)[:-1]:
+    *steps, last, _ = shared_steps(devices)
+    for bit in steps:
         if bit == half:
             low, high = parts[..., :cut], parts[..., cut:]
             mine = jnp.where(side == 0, low, high)
@@ -295,7 +298,8 @@
             mine = theirs = parts
         parts = jnp.concatenate([mine, exchange(theirs, bit)], axis=0)
         offsets += [offset ^ bit for offset in offsets]
-    far_parts = exchange(parts, 1)
+    far = exchange(parts, last)
+    shares = (parts, far, exchange(parts, 1), exchange(far, 1))
 
     ids, weights = expert_ids.T, gate_weights.T
     ids_other = exchange(ids, half)
@@ -338,9 +342,11 @@
     full = pltpu.VMEM((devices * block, cut), BF16)
     shape = jax.ShapeDtypeStruct((count, width), F32)
     shared_own, shared_other = call(
-        functools.partial(shared_kernel, offsets=tuple(offsets)),
+        functools.partial(
+            shared_kernel, offsets=tuple(offsets), hops=(0, last, 1, last ^ 1)
+        ),
         (shape, shape),
-        (me.reshape(1), parts, far_parts, normed, normed_other),
+        (me.reshape(1), *shares, normed, normed_other),
         flops=12 * count * width * cut,
         scratch_shapes=[full, full, full],
     )

time: 203 us -> 206 us (1.015)
  starting transfers between devices: 39.2 us -> 45.1 us
  local copies, waits for them, and re-layouts: 10.6 us -> 8.49 us
    ppermute x25 -> x26, waiting for transfers between devices: 119 us -> 96 us  [exchange(): return lax.ppermute(array, 'ep', [(i, i ^ bit) for i in range(devices)])]
    all_to_all x2, waiting for transfers between devices: 0.01 us -> 22 us  [within(): lax.all_to_all(array, 'ep', 0, 0, axis_index_groups=groups, tiled=True)]
    ppermute x25 -> x26, starting transfers between devices: 26.8 us -> 37.1 us  [exchange(): return lax.ppermute(array, 'ep', [(i, i ^ bit) for i in range(devices)])]
    all_to_all x2, starting transfers between devices: 12.4 us -> 8.04 us  [within(): lax.all_to_all(array, 'ep', 0, 0, axis_index_groups=groups, tiled=True)]
    unnamed x55 -> x54, local copies, waits for them, and re-layouts: 9.67 us -> 8.49 us
  transfers between devices with their start and end apart: 27 -> 28, of which waited for: 16 -> 16; matrix products, arithmetic and copies ran while one was open for 2% -> 1% of each run, Pallas kernels for 14% -> 14%
where the time goes in v4:
time: 206 us; the launch traced here: 205 us
  waiting for transfers between devices  118 us (57%)
  starting transfers between devices  45.1 us (22%)
  Pallas kernels  31.8 us (15%)
  local copies, waits for them, and re-layouts  8.49 us (4%)
    ppermute x26, waiting for transfers between devices, exchange(): return lax.ppermute(array, 'ep', [(i, i ^ bit) for i in range(devices)])  96 us
    ppermute x26, starting transfers between devices, exchange(): return lax.ppermute(array, 'ep', [(i, i ^ bit) for i in range(devices)])  37.1 us
    all_to_all x2, waiting for transfers between devices, within(): lax.all_to_all(array, 'ep', 0, 0, axis_index_groups=groups, tiled=True)  22 us
    pallas_call x2, Pallas kernels, run_experts(): pl.pallas_call(functools.partial(expert_kernel, takes=tuple(takes), resul...  20.7 us
    pallas_call x10, Pallas kernels, call(): pl.pallas_call(kernel, in_specs=[SMEM] * scalars + [VMEM] * (len(args) -...  11.2 us
    unnamed x54, local copies, waits for them, and re-layouts  8.49 us
    all_to_all x2, starting transfers between devices, within(): lax.all_to_all(array, 'ep', 0, 0, axis_index_groups=groups, tiled=True)  8.04 us
  transfers between devices with their start and end apart: 28, of which 16 were waited for; matrix products, arithmetic and copies ran while one was open for 1% of the time, Pallas kernels for 14%

profile of v4, /device:TPU:0, one launch (start us, length us, event | category | flops | bytes accessed | tf_op | source)
XLA Modules:
  0.0 205.1 jit_solution(11929475704607097638)
XLA Ops:
  2.0 4.1 %collective-permute-start.6 = (bf16[128,2048]{1,0:T(8,128)(2,1)S(1)}, bf16[128,2048]{1,0:T(8,128)(2,1)S(1)}, u32[]{:S(2)}, u32[]{:S(2)}) collective-permute-start(bf16[128,2048]{1,0:T(8,128)(2,1)S(1)} %shard_map.100.x_ref.refs_4_), channel_id=1, source_target_pairs={{0,16},{1,17},{2,18},{3,19},{4,20},{5,21},{6,22},{7,23},{8,24},{9,... | collective-permute-start | bytes 1572872 | tf_op jit(solution)/shard_map/ppermute | solution.py:270
  6.2 2.8 %collective-permute-start.24 = (f32[4,128]{1,0:T(4,128)}, f32[4,128]{1,0:T(4,128)S(1)}, u32[]{:S(2)}, u32[]{:S(2)}) collective-permute-start(f32[4,128]{1,0:T(4,128)} %bitcast.22), channel_id=1, source_target_pairs={{0,16},{1,17},{2,18},{3,19},{4,20},{5,21},{6,22},{7,23},{8,24},{9,... | collective-permute-start | bytes 6152 | tf_op jit(solution)/shard_map/ppermute | solution.py:270
  9.1 20.3 %collective-permute-done.23.ids_ref = s32[4,128]{1,0:T(4,128)S(1)} collective-permute-done((s32[4,128]{1,0:T(4,128)}, s32[4,128]{1,0:T(4,128)S(1)}, u32[]{:S(2)}, u32[]{:S(2)}) %collective-permute-start.23) | collective-permute-done | bytes 2080 | tf_op jit(solution)/shard_map/ppermute | solution.py:270
  31.1 1.7 shard_map.108
  32.9 4.1 %all-to-all-start = ((bf16[16,24,2176]{2,1,0:T(8,128)(2,1)}), bf16[16,24,2176]{2,1,0:T(8,128)(2,1)S(1)}, u32[]{:S(2)}, u32[]{:S(2)}) async-start(bf16[16,24,2176]{2,1,0:T(8,128)(2,1)} %bitcast.12), calls=%async_computation | async-start | bytes 3342336 | tf_op jit(solution)/shard_map/all_to_all | solution.py:273
  37.1 3.4 %collective-permute-start = (bf16[1,3,64,256]{3,2,1,0:T(8,128)(2,1)S(1)}, bf16[1,3,64,256]{3,2,1,0:T(8,128)(2,1)S(1)}, u32[]{:S(2)}, u32[]{:S(2)}) collective-permute-start(bf16[1,3,64,256]{3,2,1,0:T(8,128)(2,1)S(1)} %get-tuple-element.54), channel_id=1, source_target_pairs={{0,16},{1,17},{2,18},{3,19},{4,20},{5,21},{6,22},{7,23},{8,24},{9,... | collective-permute-start | bytes 294920 | tf_op jit(solution)/shard_map/ppermute | solution.py:270
  40.5 22.0 %all-to-all-done = bf16[16,24,2176]{2,1,0:T(8,128)(2,1)S(1)} async-done(((bf16[16,24,2176]{2,1,0:T(8,128)(2,1)}), bf16[16,24,2176]{2,1,0:T(8,128)(2,1)S(1)}, u32[]{:S(2)}, u32[]{:S(2)}) %all-to-all-start) | async-done | bytes 1671200 | tf_op jit(solution)/shard_map/all_to_all | solution.py:273
  63.7 10.2 %shard_map.109 = bf16[384,2048]{1,0:T(8,128)(2,1)} custom-call(bf16[2,2048,512]{2,1,0:T(8,128)(2,1)} %gate_ref.3, bf16[2,2048,512]{2,1,0:T(8,128)(2,1)} %up_ref.3, bf16[1024,2048]{1,0:T(8,128)(2,1)} %bitcast.29, bf16[384,2176]{1,0:T(8,128)(2,1)} %bitcast.24), custom_call_target="tpu_custom_call" | custom-call | flops 4831838208 | bytes 15728640 | tf_op jit(solution)/shard_map/pallas_call | solution.py:189
  73.9 3.9 %all-to-all-start.1 = ((bf16[16,24,2048]{2,1,0:T(8,128)(2,1)}), bf16[16,24,2048]{2,1,0:T(8,128)(2,1)S(1)}, u32[]{:S(2)}, u32[]{:S(2)}) async-start(bf16[16,24,2048]{2,1,0:T(8,128)(2,1)} %bitcast.25), calls=%async_computation.1 | async-start | bytes 3145728 | tf_op jit(solution)/shard_map/all_to_all | solution.py:273
  77.9 1.7 collective-permute-start.1
  81.7 1.5 collective-permute-start.7
  83.7 1.5 collective-permute-start.9
  85.2 17.1 %collective-permute-done.1 = bf16[2,3,64,256]{3,2,1,0:T(8,128)(2,1)S(1)} collective-permute-done((bf16[2,3,64,256]{3,2,1,0:T(8,128)(2,1)S(1)}, bf16[2,3,64,256]{3,2,1,0:T(8,128)(2,1)S(1)}, u32[]{:S(2)}, u32[]{:S(2)}) %collective-permute-start.1) | collective-permute-done | bytes 196640 | tf_op jit(solution)/shard_map/ppermute | solution.py:270
  103.4 1.5 collective-permute-start.10
  105.9 4.8 %collective-permute-done.8.refs_2_ = bf16[48,2176]{1,0:T(8,128)(2,1)S(1)} collective-permute-done((bf16[48,2176]{1,0:T(8,128)(2,1)S(1)}, bf16[48,2176]{1,0:T(8,128)(2,1)S(1)}, u32[]{:S(2)}, u32[]{:S(2)}) %collective-permute-start.8) | collective-permute-done | bytes 208928 | tf_op jit(solution)/shard_map/ppermute | solution.py:270
  110.7 1.5 collective-permute-start.12
  112.2 2.3 %collective-permute-start.13 = (bf16[48,2176]{1,0:T(8,128)(2,1)S(1)}, bf16[48,2176]{1,0:T(8,128)(2,1)S(1)}, u32[]{:S(2)}, u32[]{:S(2)}) collective-permute-start(bf16[48,2176]{1,0:T(8,128)(2,1)S(1)} %get-tuple-element.38), channel_id=1, source_target_pairs={{0,14},{1,15},{2,12},{3,13},{4,10},{5,11},{6,8},{7,9},{8,6},{9,7},... | collective-permute-start | bytes 626696 | tf_op jit(solution)/shard_map/ppermute | solution.py:270
  114.9 4.9 %collective-permute-done.12.refs_6_ = bf16[48,2176]{1,0:T(8,128)(2,1)S(1)} collective-permute-done((bf16[48,2176]{1,0:T(8,128)(2,1)S(1)}, bf16[48,2176]{1,0:T(8,128)(2,1)S(1)}, u32[]{:S(2)}, u32[]{:S(2)}) %collective-permute-start.12) | collective-permute-done | bytes 208928 | tf_op jit(solution)/shard_map/ppermute | solution.py:270
  119.8 4.4 %collective-permute-done.13.refs_7_ = bf16[48,2176]{1,0:T(8,128)(2,1)S(1)} collective-permute-done((bf16[48,2176]{1,0:T(8,128)(2,1)S(1)}, bf16[48,2176]{1,0:T(8,128)(2,1)S(1)}, u32[]{:S(2)}, u32[]{:S(2)}) %collective-permute-start.13) | collective-permute-done | bytes 208928 | tf_op jit(solution)/shard_map/ppermute | solution.py:270
  124.4 2.0 collective-permute-done.2
  127.8 18.8 %collective-permute-done.3.refs_1_ = bf16[8,3,64,256]{3,2,1,0:T(8,128)(2,1)} collective-permute-done((bf16[8,3,64,256]{3,2,1,0:T(8,128)(2,1)S(1)}, bf16[8,3,64,256]{3,2,1,0:T(8,128)(2,1)}, u32[]{:S(2)}, u32[]{:S(2)}) %collective-permute-start.3) | collective-permute-done | bytes 786464 | tf_op jit(solution)/shard_map/ppermute | solution.py:270
  146.6 10.5 %shard_map.104 = (bf16[192,2048]{1,0:T(8,128)(2,1)}, bf16[192,2048]{1,0:T(8,128)(2,1)}) custom-call(bf16[2,2048,512]{2,1,0:T(8,128)(2,1)} %gate_ref.3, bf16[2,2048,512]{2,1,0:T(8,128)(2,1)} %up_ref.3, bf16[1024,2048]{1,0:T(8,128)(2,1)} %bitcast.30, bf16[48,2176]{1,0:T(8,128)(2,1)} %copy-done.6, bf16[48,2176]{1,0:T(8,128)(2,1)} %copy-done.7, ...), custom_call_target="tpu_custom_call" | custom-call | flops 4831838208 | bytes 15728640 | tf_op jit(solution)/shard_map/pallas_call | solution.py:189
  157.7 3.3 %shard_map.102 = (f32[128,2048]{1,0:T(8,128)S(1)}, f32[128,2048]{1,0:T(8,128)S(1)}) custom-call(s32[1]{0:T(128)} %bitcast.5.me_ref, bf16[8,3,64,256]{3,2,1,0:T(8,128)(2,1)S(1)} %pad_maximum_fusion.refs_0_, bf16[8,3,64,256]{3,2,1,0:T(8,128)(2,1)} %collective-permute-done.3.refs_1_, bf16[8,3,64,256]{3,2,1,0:T(8,128)(2,1)} %collective-permute-done.4.refs_2_, ...), custom_call_target="tpu_custom_call" | custom-call | flops 805306368 | bytes 6291460 | tf_op jit(solution)/shard_map/pallas_call | solution.py:230
  165.9 3.4 %collective-permute-start.25 = (bf16[128,2048]{1,0:T(8,128)(2,1)S(1)}, bf16[128,2048]{1,0:T(8,128)(2,1)S(1)}, u32[]{:S(2)}, u32[]{:S(2)}) collective-permute-start(bf16[128,2048]{1,0:T(8,128)(2,1)S(1)} %shard_map.110), channel_id=1, source_target_pairs={{0,16},{1,17},{2,18},{3,19},{4,20},{5,21},{6,22},{7,23},{8,24},{9,... | collective-permute-start | bytes 1572872 | tf_op jit(solution)/shard_map/ppermute | solution.py:270
  170.6 2.1 %collective-permute-start.17 = (bf16[48,2048]{1,0:T(8,128)(2,1)S(1)}, bf16[48,2048]{1,0:T(8,128)(2,1)S(1)}, u32[]{:S(2)}, u32[]{:S(2)}) collective-permute-start(bf16[48,2048]{1,0:T(8,128)(2,1)S(1)} %get-tuple-element.43), channel_id=1, source_target_pairs={{0,4},{1,5},{2,6},{3,7},{4,0},{5,1},{6,2},{7,3},{8,12},{9,13},{10,... | collective-permute-start | bytes 589832 | tf_op jit(solution)/shard_map/ppermute | solution.py:270
  172.7 1.4 collective-permute-start.18
  175.1 3.3 %collective-permute-done.16.refs_1_ = bf16[48,2048]{1,0:T(8,128)(2,1)S(1)} collective-permute-done((bf16[48,2048]{1,0:T(8,128)(2,1)S(1)}, bf16[48,2048]{1,0:T(8,128)(2,1)S(1)}, u32[]{:S(2)}, u32[]{:S(2)}) %collective-permute-start.16) | collective-permute-done | bytes 196640 | tf_op jit(solution)/shard_map/ppermute | solution.py:270
  180.1 4.3 %collective-permute-start.21 = (bf16[48,2048]{1,0:T(8,128)(2,1)S(1)}, bf16[48,2048]{1,0:T(8,128)(2,1)S(1)}, u32[]{:S(2)}, u32[]{:S(2)}) collective-permute-start(bf16[48,2048]{1,0:T(8,128)(2,1)S(1)} %get-tuple-element.47), channel_id=1, source_target_pairs={{0,12},{1,13},{2,14},{3,15},{4,8},{5,9},{6,10},{7,11},{8,4},{9,5},... | collective-permute-start | bytes 589832 | tf_op jit(solution)/shard_map/ppermute | solution.py:270
  184.4 1.5 collective-permute-done.19.refs_4_
  185.9 10.4 %collective-permute-done.20.refs_5_ = bf16[48,2048]{1,0:T(8,128)(2,1)S(1)} collective-permute-done((bf16[48,2048]{1,0:T(8,128)(2,1)S(1)}, bf16[48,2048]{1,0:T(8,128)(2,1)S(1)}, u32[]{:S(2)}, u32[]{:S(2)}) %collective-permute-start.20) | collective-permute-done | bytes 196640 | tf_op jit(solution)/shard_map/ppermute | solution.py:270
  196.3 4.3 %collective-permute-done.21.refs_6_ = bf16[48,2048]{1,0:T(8,128)(2,1)S(1)} collective-permute-done((bf16[48,2048]{1,0:T(8,128)(2,1)S(1)}, bf16[48,2048]{1,0:T(8,128)(2,1)S(1)}, u32[]{:S(2)}, u32[]{:S(2)}) %collective-permute-start.21) | collective-permute-done | bytes 196640 | tf_op jit(solution)/shard_map/ppermute | solution.py:270
  200.6 2.9 %collective-permute-done.22.refs_7_ = bf16[48,2048]{1,0:T(8,128)(2,1)S(1)} collective-permute-done((bf16[48,2048]{1,0:T(8,128)(2,1)S(1)}, bf16[48,2048]{1,0:T(8,128)(2,1)S(1)}, u32[]{:S(2)}, u32[]{:S(2)}) %collective-permute-start.22) | collective-permute-done | bytes 196640 | tf_op jit(solution)/shard_map/ppermute | solution.py:270
  (97 shorter events, 22.9 us)
Async XLA Ops:
  2.0 29.2 %collective-permute-start.6 = (bf16[128,2048]{1,0:T(8,128)(2,1)S(1)}, bf16[128,2048]{1,0:T(8,128)(2,1)S(1)}, u32[]{:S(2)}, u32[]{:S(2)}) collective-permute-start(bf16[128,2048]{1,0:T(8,128)(2,1)S(1)} %shard_map.100.x_ref.refs_4_), channel_id=1, source_target_pairs={{0,16},{1,17},{2,18},{3,19},{4,20},{5,21},{6,22},{7,23},{8,24},{9,... | collective-permute-start | bytes 1572872 | tf_op jit(solution)/shard_map/ppermute | solution.py:270
  6.1 23.3 %collective-permute-start.23 = (s32[4,128]{1,0:T(4,128)}, s32[4,128]{1,0:T(4,128)S(1)}, u32[]{:S(2)}, u32[]{:S(2)}) collective-permute-start(s32[4,128]{1,0:T(4,128)} %bitcast.20), channel_id=1, source_target_pairs={{0,16},{1,17},{2,18},{3,19},{4,20},{5,21},{6,22},{7,23},{8,24},{9,... | collective-permute-start | bytes 6152 | tf_op jit(solution)/shard_map/ppermute | solution.py:270
  6.2 23.3 %collective-permute-start.24 = (f32[4,128]{1,0:T(4,128)}, f32[4,128]{1,0:T(4,128)S(1)}, u32[]{:S(2)}, u32[]{:S(2)}) collective-permute-start(f32[4,128]{1,0:T(4,128)} %bitcast.22), channel_id=1, source_target_pairs={{0,16},{1,17},{2,18},{3,19},{4,20},{5,21},{6,22},{7,23},{8,24},{9,... | collective-permute-start | bytes 6152 | tf_op jit(solution)/shard_map/ppermute | solution.py:270
  32.9 29.7 %all-to-all-start = ((bf16[16,24,2176]{2,1,0:T(8,128)(2,1)}), bf16[16,24,2176]{2,1,0:T(8,128)(2,1)S(1)}, u32[]{:S(2)}, u32[]{:S(2)}) async-start(bf16[16,24,2176]{2,1,0:T(8,128)(2,1)} %bitcast.12), calls=%async_computation | async-start | bytes 3342336 | tf_op jit(solution)/shard_map/all_to_all | solution.py:273
  37.1 40.7 %collective-permute-start = (bf16[1,3,64,256]{3,2,1,0:T(8,128)(2,1)S(1)}, bf16[1,3,64,256]{3,2,1,0:T(8,128)(2,1)S(1)}, u32[]{:S(2)}, u32[]{:S(2)}) collective-permute-start(bf16[1,3,64,256]{3,2,1,0:T(8,128)(2,1)S(1)} %get-tuple-element.54), channel_id=1, source_target_pairs={{0,16},{1,17},{2,18},{3,19},{4,20},{5,21},{6,22},{7,23},{8,24},{9,... | collective-permute-start | bytes 294920 | tf_op jit(solution)/shard_map/ppermute | solution.py:270
  73.9 89.1 %all-to-all-start.1 = ((bf16[16,24,2048]{2,1,0:T(8,128)(2,1)}), bf16[16,24,2048]{2,1,0:T(8,128)(2,1)S(1)}, u32[]{:S(2)}, u32[]{:S(2)}) async-start(bf16[16,24,2048]{2,1,0:T(8,128)(2,1)} %bitcast.25), calls=%async_computation.1 | async-start | bytes 3145728 | tf_op jit(solution)/shard_map/all_to_all | solution.py:273
  77.9 46.5 %copy-start.22 = (bf16[1,3,64,256]{3,2,1,0:T(8,128)(2,1)}, bf16[1,3,64,256]{3,2,1,0:T(8,128)(2,1)S(1)}, u32[]{:S(2)}) copy-start(bf16[1,3,64,256]{3,2,1,0:T(8,128)(2,1)S(1)} %collective-permute-done) | copy-start | bytes 294916
  77.9 24.4 %collective-permute-start.1 = (bf16[2,3,64,256]{3,2,1,0:T(8,128)(2,1)S(1)}, bf16[2,3,64,256]{3,2,1,0:T(8,128)(2,1)S(1)}, u32[]{:S(2)}, u32[]{:S(2)}) collective-permute-start(bf16[2,3,64,256]{3,2,1,0:T(8,128)(2,1)S(1)} %pad_maximum_fusion.2), channel_id=1, source_target_pairs={{0,4},{1,5},{2,6},{3,7},{4,0},{5,1},{6,2},{7,3},{8,12},{9,13},{10,... | collective-permute-start | bytes 589832 | tf_op jit(solution)/shard_map/ppermute | solution.py:270
  81.7 45.7 %copy-start.6 = (bf16[48,2176]{1,0:T(8,128)(2,1)}, bf16[48,2176]{1,0:T(8,128)(2,1)S(1)}, u32[]{:S(2)}) copy-start(bf16[48,2176]{1,0:T(8,128)(2,1)S(1)} %get-tuple-element.31.refs_0_) | copy-start | bytes 626692
  81.7 23.3 %collective-permute-start.7 = (bf16[48,2176]{1,0:T(8,128)(2,1)S(1)}, bf16[48,2176]{1,0:T(8,128)(2,1)S(1)}, u32[]{:S(2)}, u32[]{:S(2)}) collective-permute-start(bf16[48,2176]{1,0:T(8,128)(2,1)S(1)} %get-tuple-element.32), channel_id=1, source_target_pairs={{0,2},{1,3},{2,0},{3,1},{4,6},{5,7},{6,4},{7,5},{8,10},{9,11},{10,... | collective-permute-start | bytes 626696 | tf_op jit(solution)/shard_map/ppermute | solution.py:270
  83.2 27.5 %collective-permute-start.8 = (bf16[48,2176]{1,0:T(8,128)(2,1)S(1)}, bf16[48,2176]{1,0:T(8,128)(2,1)S(1)}, u32[]{:S(2)}, u32[]{:S(2)}) collective-permute-start(bf16[48,2176]{1,0:T(8,128)(2,1)S(1)} %get-tuple-element.33), channel_id=1, source_target_pairs={{0,4},{1,5},{2,6},{3,7},{4,0},{5,1},{6,2},{7,3},{8,12},{9,13},{10,... | collective-permute-start | bytes 626696 | tf_op jit(solution)/shard_map/ppermute | solution.py:270
  83.7 28.5 %collective-permute-start.9 = (bf16[48,2176]{1,0:T(8,128)(2,1)S(1)}, bf16[48,2176]{1,0:T(8,128)(2,1)S(1)}, u32[]{:S(2)}, u32[]{:S(2)}) collective-permute-start(bf16[48,2176]{1,0:T(8,128)(2,1)S(1)} %get-tuple-element.34), channel_id=1, source_target_pairs={{0,6},{1,7},{2,4},{3,5},{4,2},{5,3},{6,0},{7,1},{8,14},{9,15},{10,... | collective-permute-start | bytes 626696 | tf_op jit(solution)/shard_map/ppermute | solution.py:270
  102.3 24.0 %collective-permute-start.2 = (bf16[4,3,64,256]{3,2,1,0:T(8,128)(2,1)S(1)}, bf16[4,3,64,256]{3,2,1,0:T(8,128)(2,1)S(1)}, u32[]{:S(2)}, u32[]{:S(2)}) collective-permute-start(bf16[4,3,64,256]{3,2,1,0:T(8,128)(2,1)S(1)} %pad_maximum_fusion.1), channel_id=1, source_target_pairs={{0,2},{1,3},{2,0},{3,1},{4,6},{5,7},{6,4},{7,5},{8,10},{9,11},{10,... | collective-permute-start | bytes 1179656 | tf_op jit(solution)/shard_map/ppermute | solution.py:270
  103.4 11.2 %collective-permute-start.10 = (bf16[48,2176]{1,0:T(8,128)(2,1)S(1)}, bf16[48,2176]{1,0:T(8,128)(2,1)S(1)}, u32[]{:S(2)}, u32[]{:S(2)}) collective-permute-start(bf16[48,2176]{1,0:T(8,128)(2,1)S(1)} %get-tuple-element.35), channel_id=1, source_target_pairs={{0,8},{1,9},{2,10},{3,11},{4,12},{5,13},{6,14},{7,15},{8,0},{9,1},... | collective-permute-start | bytes 626696 | tf_op jit(solution)/shard_map/ppermute | solution.py:270
  105.0 9.9 %collective-permute-start.11 = (bf16[48,2176]{1,0:T(8,128)(2,1)S(1)}, bf16[48,2176]{1,0:T(8,128)(2,1)S(1)}, u32[]{:S(2)}, u32[]{:S(2)}) collective-permute-start(bf16[48,2176]{1,0:T(8,128)(2,1)S(1)} %get-tuple-element.36), channel_id=1, source_target_pairs={{0,10},{1,11},{2,8},{3,9},{4,14},{5,15},{6,12},{7,13},{8,2},{9,3},... | collective-permute-start | bytes 626696 | tf_op jit(solution)/shard_map/ppermute | solution.py:270
  110.7 9.1 %collective-permute-start.12 = (bf16[48,2176]{1,0:T(8,128)(2,1)S(1)}, bf16[48,2176]{1,0:T(8,128)(2,1)S(1)}, u32[]{:S(2)}, u32[]{:S(2)}) collective-permute-start(bf16[48,2176]{1,0:T(8,128)(2,1)S(1)} %get-tuple-element.37), channel_id=1, source_target_pairs={{0,12},{1,13},{2,14},{3,15},{4,8},{5,9},{6,10},{7,11},{8,4},{9,5},... | collective-permute-start | bytes 626696 | tf_op jit(solution)/shard_map/ppermute | solution.py:270
  112.2 12.0 %collective-permute-start.13 = (bf16[48,2176]{1,0:T(8,128)(2,1)S(1)}, bf16[48,2176]{1,0:T(8,128)(2,1)S(1)}, u32[]{:S(2)}, u32[]{:S(2)}) collective-permute-start(bf16[48,2176]{1,0:T(8,128)(2,1)S(1)} %get-tuple-element.38), channel_id=1, source_target_pairs={{0,14},{1,15},{2,12},{3,13},{4,10},{5,11},{6,8},{7,9},{8,6},{9,7},... | collective-permute-start | bytes 626696 | tf_op jit(solution)/shard_map/ppermute | solution.py:270
  124.3 22.4 %collective-permute-start.14 = (bf16[192,2176]{1,0:T(8,128)(2,1)S(1)}, bf16[192,2176]{1,0:T(8,128)(2,1)}, u32[]{:S(2)}, u32[]{:S(2)}) collective-permute-start(bf16[192,2176]{1,0:T(8,128)(2,1)S(1)} %shard_map.103), channel_id=1, source_target_pairs={{0,1},{1,0},{2,3},{3,2},{4,5},{5,4},{6,7},{7,6},{8,9},{9,8},{10,11... | collective-permute-start | bytes 2506760 | tf_op jit(solution)/shard_map/ppermute | solution.py:270
  127.5 19.2 %collective-permute-start.3 = (bf16[8,3,64,256]{3,2,1,0:T(8,128)(2,1)S(1)}, bf16[8,3,64,256]{3,2,1,0:T(8,128)(2,1)}, u32[]{:S(2)}, u32[]{:S(2)}) collective-permute-start(bf16[8,3,64,256]{3,2,1,0:T(8,128)(2,1)S(1)} %pad_maximum_fusion.refs_0_), channel_id=1, source_target_pairs={{0,8},{1,9},{2,10},{3,11},{4,12},{5,13},{6,14},{7,15},{8,0},{9,1},... | collective-permute-start | bytes 2359304 | tf_op jit(solution)/shard_map/ppermute | solution.py:270
  127.8 29.9 %collective-permute-start.4 = (bf16[8,3,64,256]{3,2,1,0:T(8,128)(2,1)S(1)}, bf16[8,3,64,256]{3,2,1,0:T(8,128)(2,1)}, u32[]{:S(2)}, u32[]{:S(2)}) collective-permute-start(bf16[8,3,64,256]{3,2,1,0:T(8,128)(2,1)S(1)} %pad_maximum_fusion.refs_0_), channel_id=1, source_target_pairs={{0,1},{1,0},{2,3},{3,2},{4,5},{5,4},{6,7},{7,6},{8,9},{9,8},{10,11... | collective-permute-start | bytes 2359304 | tf_op jit(solution)/shard_map/ppermute | solution.py:270
  146.6 11.1 %collective-permute-start.5 = (bf16[8,3,64,256]{3,2,1,0:T(8,128)(2,1)}, bf16[8,3,64,256]{3,2,1,0:T(8,128)(2,1)}, u32[]{:S(2)}, u32[]{:S(2)}) collective-permute-start(bf16[8,3,64,256]{3,2,1,0:T(8,128)(2,1)} %collective-permute-done.3.refs_1_), channel_id=1, source_target_pairs={{0,1},{1,0},{2,3},{3,2},{4,5},{5,4},{6,7},{7,6},{8,9},{9,8},{10,11... | collective-permute-start | bytes 2359304 | tf_op jit(solution)/shard_map/ppermute | solution.py:270
  157.1 12.2 %collective-permute-start.15 = (bf16[192,2048]{1,0:T(8,128)(2,1)}, bf16[192,2048]{1,0:T(8,128)(2,1)}, u32[]{:S(2)}, u32[]{:S(2)}) collective-permute-start(bf16[192,2048]{1,0:T(8,128)(2,1)} %get-tuple-element.40), channel_id=1, source_target_pairs={{0,1},{1,0},{2,3},{3,2},{4,5},{5,4},{6,7},{7,6},{8,9},{9,8},{10,11... | collective-permute-start | bytes 2359304 | tf_op jit(solution)/shard_map/ppermute | solution.py:270
  165.2 38.3 %copy-start.3 = (f32[128,2048]{1,0:T(8,128)S(1)}, f32[128,2048]{1,0:T(8,128)}, u32[]{:S(2)}) copy-start(f32[128,2048]{1,0:T(8,128)} %copy-done.2) | copy-start | bytes 3145732
  165.2 38.3 %copy-start.17 = (bf16[256,384]{1,0:T(8,128)(2,1)S(1)}, bf16[256,384]{1,0:T(8,128)(2,1)}, u32[]{:S(2)}) copy-start(bf16[256,384]{1,0:T(8,128)(2,1)} %copy-done.16) | copy-start | bytes 589828
  165.9 38.3 %collective-permute-start.25 = (bf16[128,2048]{1,0:T(8,128)(2,1)S(1)}, bf16[128,2048]{1,0:T(8,128)(2,1)S(1)}, u32[]{:S(2)}, u32[]{:S(2)}) collective-permute-start(bf16[128,2048]{1,0:T(8,128)(2,1)S(1)} %shard_map.110), channel_id=1, source_target_pairs={{0,16},{1,17},{2,18},{3,19},{4,20},{5,21},{6,22},{7,23},{8,24},{9,... | collective-permute-start | bytes 1572872 | tf_op jit(solution)/shard_map/ppermute | solution.py:270
  170.5 7.8 %collective-permute-start.16 = (bf16[48,2048]{1,0:T(8,128)(2,1)S(1)}, bf16[48,2048]{1,0:T(8,128)(2,1)S(1)}, u32[]{:S(2)}, u32[]{:S(2)}) collective-permute-start(bf16[48,2048]{1,0:T(8,128)(2,1)S(1)} %get-tuple-element.42), channel_id=1, source_target_pairs={{0,2},{1,3},{2,0},{3,1},{4,6},{5,7},{6,4},{7,5},{8,10},{9,11},{10,... | collective-permute-start | bytes 589832 | tf_op jit(solution)/shard_map/ppermute | solution.py:270
  170.6 9.5 %collective-permute-start.17 = (bf16[48,2048]{1,0:T(8,128)(2,1)S(1)}, bf16[48,2048]{1,0:T(8,128)(2,1)S(1)}, u32[]{:S(2)}, u32[]{:S(2)}) collective-permute-start(bf16[48,2048]{1,0:T(8,128)(2,1)S(1)} %get-tuple-element.43), channel_id=1, source_target_pairs={{0,4},{1,5},{2,6},{3,7},{4,0},{5,1},{6,2},{7,3},{8,12},{9,13},{10,... | collective-permute-start | bytes 589832 | tf_op jit(solution)/shard_map/ppermute | solution.py:270
  172.7 11.7 %collective-permute-start.18 = (bf16[48,2048]{1,0:T(8,128)(2,1)S(1)}, bf16[48,2048]{1,0:T(8,128)(2,1)S(1)}, u32[]{:S(2)}, u32[]{:S(2)}) collective-permute-start(bf16[48,2048]{1,0:T(8,128)(2,1)S(1)} %get-tuple-element.44), channel_id=1, source_target_pairs={{0,6},{1,7},{2,4},{3,5},{4,2},{5,3},{6,0},{7,1},{8,14},{9,15},{10,... | collective-permute-start | bytes 589832 | tf_op jit(solution)/shard_map/ppermute | solution.py:270
  174.1 11.8 %collective-permute-start.19 = (bf16[48,2048]{1,0:T(8,128)(2,1)S(1)}, bf16[48,2048]{1,0:T(8,128)(2,1)S(1)}, u32[]{:S(2)}, u32[]{:S(2)}) collective-permute-start(bf16[48,2048]{1,0:T(8,128)(2,1)S(1)} %get-tuple-element.45), channel_id=1, source_target_pairs={{0,8},{1,9},{2,10},{3,11},{4,12},{5,13},{6,14},{7,15},{8,0},{9,1},... | collective-permute-start | bytes 589832 | tf_op jit(solution)/shard_map/ppermute | solution.py:270
  178.4 17.9 %collective-permute-start.20 = (bf16[48,2048]{1,0:T(8,128)(2,1)S(1)}, bf16[48,2048]{1,0:T(8,128)(2,1)S(1)}, u32[]{:S(2)}, u32[]{:S(2)}) collective-permute-start(bf16[48,2048]{1,0:T(8,128)(2,1)S(1)} %get-tuple-element.46), channel_id=1, source_target_pairs={{0,10},{1,11},{2,8},{3,9},{4,14},{5,15},{6,12},{7,13},{8,2},{9,3},... | collective-permute-start | bytes 589832 | tf_op jit(solution)/shard_map/ppermute | solution.py:270
  180.1 20.4 %collective-permute-start.21 = (bf16[48,2048]{1,0:T(8,128)(2,1)S(1)}, bf16[48,2048]{1,0:T(8,128)(2,1)S(1)}, u32[]{:S(2)}, u32[]{:S(2)}) collective-permute-start(bf16[48,2048]{1,0:T(8,128)(2,1)S(1)} %get-tuple-element.47), channel_id=1, source_target_pairs={{0,12},{1,13},{2,14},{3,15},{4,8},{5,9},{6,10},{7,11},{8,4},{9,5},... | collective-permute-start | bytes 589832 | tf_op jit(solution)/shard_map/ppermute | solution.py:270
  184.4 19.1 %collective-permute-start.22 = (bf16[48,2048]{1,0:T(8,128)(2,1)S(1)}, bf16[48,2048]{1,0:T(8,128)(2,1)S(1)}, u32[]{:S(2)}, u32[]{:S(2)}) collective-permute-start(bf16[48,2048]{1,0:T(8,128)(2,1)S(1)} %get-tuple-element.48), channel_id=1, source_target_pairs={{0,14},{1,15},{2,12},{3,13},{4,10},{5,11},{6,8},{7,9},{8,6},{9,7},... | collective-permute-start | bytes 589832 | tf_op jit(solution)/shard_map/ppermute | solution.py:270
  (23 other events, 149.5 us)
